TPU v7x, 32 devices: a whole 2x2x4 slice. The times are simulated.
32 devices in a mesh: sp: 8 (over z, y), tp: 4 (over x, core).
Axes of the slice: x: 2, y: 2, z: 4, core: 2. Of those that a mesh axis runs over, the one named last changes fastest.
Arguments:
- tokens: bfloat16 [4096, 2048], P(('sp', 'tp')), may hold values from -6 to 6
- norm_gain: float32 [2048], replicated, may hold values from 0.1 to 1.9
- query_weight: bfloat16 [2048, 2048], P('sp', 'tp'), may hold values from -0.125 to 0.125
- key_weight: bfloat16 [2048, 2048], P('sp', 'tp'), may hold values from -0.125 to 0.125
- value_weight: bfloat16 [2048, 4096], P('sp', 'tp'), may hold values from -0.125 to 0.125
- retain_gate: bfloat16 [2048, 4096], P('sp', 'tp'), may hold values from -0.125 to 0.125
- unit_value: bfloat16 [2048, 2048], P('sp', 'tp'), may hold values from -0.125 to 0.125
- unit_gate: bfloat16 [2048, 2048], P('sp', 'tp'), may hold values from -0.125 to 0.125
- convolve_gate: bfloat16 [2048, 2048], P('sp', 'tp'), may hold values from -0.125 to 0.125
- filter_taps: float32 [31, 2048], replicated, may hold values from -1 to 1
- layer_gain: float32 [2048], replicated, may hold values from 0.1 to 1.9
- layer_shift: float32 [2048], replicated, may hold values from -3 to 3
- retain_output: bfloat16 [2048, 4096], P('sp', 'tp'), may hold values from -0.09375 to 0.09375
- convolve_output: bfloat16 [2048, 2048], P('sp', 'tp'), may hold values from -0.125 to 0.125
Outputs:
- mixed: bfloat16 [4096, 2048], P(('sp', 'tp'))
All inputs are finite; a program needn't handle non-finite values.
Results may differ from a plain program's by a relative error of at most 0.018.
Values may be sent and summed in bfloat16 or wider, within the bound.
No kernel may reach another device: no remote copies, remote signals or barrier semaphores. Data moves between devices by JAX's collectives and lax.ppermute only.
A program may use at most 128 MiB of HBM per device.

v0:
```python
import jax
import jax.numpy as jnp
from jax import lax
from jax.sharding import PartitionSpec as P

KEY = 256
VAL = 512
GROUP = 512
KW = 31


rms_eps = 1e-06
group_eps = 1.0
layer_eps = 0.001
rope_base = 10000.0
highest = lax.Precision.HIGHEST


def carried_in(part, axis, combine, identity):
    place = lax.axis_index(axis)
    gathered = jax.tree.map(lambda a: lax.all_gather(a, axis), part)
    state = jax.tree.map(lambda a, e: jnp.zeros_like(a) + jnp.asarray(e, a.dtype), part, identity)

    def one(hop, state):
        return combine(
            state, jax.tree.map(lambda a: lax.dynamic_index_in_dim(a, hop, 0, False), gathered)
        )

    return lax.fori_loop(0, place, one, state)


def from_behind(x, axis, by):
    length = lax.axis_size(axis)
    pairs = [(i, i + by) for i in range(length) if 0 <= i + by < length]
    return lax.ppermute(x, axis, pairs)


def rms_normalize(tokens, norm_gain):
    widened = tokens.astype(jnp.float32)
    scaled = widened * lax.rsqrt(jnp.mean(widened * widened, axis=-1, keepdims=True) + rms_eps)
    return (scaled * norm_gain).astype(jnp.bfloat16)


def rotate(vectors, positions):
    half_width = vectors.shape[-1] // 2
    frequency = rope_base ** (-jnp.arange(half_width, dtype=jnp.float32) / half_width)
    angles = positions.astype(jnp.float32)[:, None] * frequency
    cosine = jnp.cos(angles)[:, None, :]
    sine_part = jnp.sin(angles)[:, None, :]
    front_half = vectors[..., :half_width]
    back_half = vectors[..., half_width:]
    return jnp.concatenate(
        [front_half * cosine - back_half * sine_part, front_half * sine_part + back_half * cosine],
        axis=-1,
    )


def prepare(queries, key_rows, values, positions):
    row_count = queries.shape[0]
    rotated_query = rotate(
        queries.astype(jnp.float32).reshape(row_count, -1, KEY), positions
    ).astype(jnp.bfloat16)
    rotated_keys = (
        rotate(key_rows.astype(jnp.float32).reshape(row_count, -1, KEY), positions) * KEY ** (-0.5)
    ).astype(jnp.bfloat16)
    value_heads = values.reshape(row_count, -1, VAL)
    return (rotated_query, rotated_keys, value_heads)


def decay_logs(first_head, head_total, all_heads, seq_length):
    ratio = (first_head + jnp.arange(head_total)).astype(jnp.float32) / (all_heads - 1)
    return (jnp.log(0.05) + ratio * jnp.log(18.0)) / seq_length


def local_parts(queries, key_rows, values, log_decay):
    row_count = queries.shape[0]
    indices = jnp.arange(row_count, dtype=jnp.float32)
    offsets = indices[:, None] - indices[None, :]
    causal = offsets >= 0
    weight = jnp.where(
        causal[None], jnp.exp(log_decay[:, None, None] * jnp.where(causal, offsets, 0.0)[None]), 0.0
    )
    scores = (
        jnp.einsum("ihd,jhd->hij", queries, key_rows, preferred_element_type=jnp.float32) * weight
    ).astype(jnp.bfloat16)
    within = jnp.einsum("hij,jhe->ihe", scores, values, preferred_element_type=jnp.float32)
    trailing = jnp.exp(log_decay[None, :] * (row_count - 1.0 - indices)[:, None])
    weighted = (key_rows.astype(jnp.float32) * trailing[:, :, None]).astype(jnp.bfloat16)
    contribution = jnp.einsum("jhd,jhe->hde", weighted, values, preferred_element_type=jnp.float32)
    return (within, contribution)


def cross_part(queries, carry_state, log_decay):
    row_count = queries.shape[0]
    indices = jnp.arange(row_count, dtype=jnp.float32)
    leading = jnp.exp(log_decay[None, :] * (indices + 1.0)[:, None])
    return (
        jnp.einsum("ihd,hde->ihe", queries.astype(jnp.float32), carry_state, precision=highest)
        * leading[:, :, None]
    )


def retain_finish(raw, switch):
    average = jnp.mean(raw, axis=-1, keepdims=True)
    spread = jnp.mean(jnp.square(raw - average), axis=-1, keepdims=True)
    normalized = ((raw - average) * lax.rsqrt(spread + group_eps)).reshape(raw.shape[0], -1)
    return (normalized * jax.nn.silu(switch.astype(jnp.float32))).astype(jnp.bfloat16)


def convolve_branch(gated_input, before, tap_slice, gain_slice, shift_slice, switch):
    padded = jnp.concatenate([before, gated_input], axis=0)
    row_count = gated_input.shape[0]
    summed = jnp.zeros(gated_input.shape, jnp.float32)
    for tap_index in range(tap_slice.shape[0]):
        summed = (
            summed
            + padded[tap_index : tap_index + row_count].astype(jnp.float32) * tap_slice[tap_index]
        )
    grouped = summed.reshape(row_count, -1, GROUP)
    average = jnp.mean(grouped, axis=-1, keepdims=True)
    spread = jnp.mean(jnp.square(grouped - average), axis=-1, keepdims=True)
    normalized = ((grouped - average) * lax.rsqrt(spread + layer_eps)).reshape(row_count, -1)
    normalized = normalized * gain_slice + shift_slice
    return (jax.nn.silu(normalized) * jax.nn.silu(switch.astype(jnp.float32))).astype(jnp.bfloat16)


def contract(hidden, matrix):
    return lax.dot_general(
        hidden, matrix, (((1,), (1,)), ((), ())), preferred_element_type=jnp.float32
    )


def join_states(earlier, later):
    return (earlier[0] * later[0], later[0][:, None, None] * earlier[1] + later[1])


def local(
    tokens,
    norm_gain,
    query_weight,
    key_weight,
    value_weight,
    retain_gate,
    unit_value,
    unit_gate,
    convolve_gate,
    filter_taps,
    layer_gain,
    layer_shift,
    retain_output,
    convolve_output,
):
    head_groups = lax.axis_size("tp")
    chain_length = lax.axis_size("sp")
    head_rank = lax.axis_index("tp")
    chain_rank = lax.axis_index("sp")
    normed = rms_normalize(tokens, norm_gain)
    gathered = (
        lax.all_gather(query_weight, "sp", axis=0, tiled=True),
        lax.all_gather(key_weight, "sp", axis=0, tiled=True),
        lax.all_gather(value_weight, "sp", axis=0, tiled=True),
        lax.all_gather(retain_gate, "sp", axis=0, tiled=True),
        lax.all_gather(unit_value, "sp", axis=0, tiled=True),
        lax.all_gather(unit_gate, "sp", axis=0, tiled=True),
        lax.all_gather(convolve_gate, "sp", axis=0, tiled=True),
        lax.all_gather(retain_output, "sp", axis=0, tiled=True),
        lax.all_gather(convolve_output, "sp", axis=0, tiled=True),
    )
    in_weights = gathered[:7]
    retain_full = gathered[7]
    convolve_full = gathered[8]

    def project(row_piece):
        return jnp.concatenate(
            [
                jnp.dot(row_piece, matrix, preferred_element_type=jnp.float32).astype(jnp.bfloat16)
                for matrix in in_weights
            ],
            axis=1,
        )

    projected = project(lax.all_gather(normed, "tp", axis=0, tiled=True))
    row_count = projected.shape[0]
    bounds = [0]
    for matrix in in_weights:
        bounds.append(bounds[-1] + matrix.shape[1])
    pieces = [projected[:, bounds[column] : bounds[column + 1]] for column in range(7)]
    queries, key_rows, values, retain_switch, glu_value, glu_switch, convolve_switch = pieces
    local_heads = queries.shape[1] // KEY
    positions = chain_rank * row_count + jnp.arange(row_count, dtype=jnp.int32)
    rotated_query, rotated_keys, value_heads = prepare(queries, key_rows, values, positions)
    log_decay = decay_logs(
        head_rank * local_heads, local_heads, local_heads * head_groups, row_count * chain_length
    )
    within, contribution = local_parts(rotated_query, rotated_keys, value_heads, log_decay)
    totals = jnp.exp(log_decay * row_count)
    gated_input = (
        glu_value.astype(jnp.float32) * jax.nn.sigmoid(glu_switch.astype(jnp.float32))
    ).astype(jnp.bfloat16)
    channels = gated_input.shape[1]
    before = from_behind(gated_input[row_count - (KW - 1) :], "sp", 1)
    prefix = carried_in(
        (totals, contribution),
        "sp",
        join_states,
        (jnp.ones_like(totals), jnp.zeros_like(contribution)),
    )
    incoming = prefix[1]
    raw = within + cross_part(rotated_query, incoming, log_decay)
    retain_hidden = retain_finish(raw, retain_switch)
    tap_slice = lax.dynamic_slice_in_dim(filter_taps, head_rank * channels, channels, 1)
    gain_slice = lax.dynamic_slice_in_dim(layer_gain, head_rank * channels, channels, 0)
    shift_slice = lax.dynamic_slice_in_dim(layer_shift, head_rank * channels, channels, 0)
    convolve_hidden = convolve_branch(
        gated_input, before, tap_slice, gain_slice, shift_slice, convolve_switch
    )
    return lax.psum_scatter(
        (contract(retain_hidden, retain_full) + contract(convolve_hidden, convolve_full)).astype(
            jnp.bfloat16
        ),
        "tp",
        scatter_dimension=0,
        tiled=True,
    )


def solution(mesh):
    return jax.shard_map(
        local,
        mesh=mesh,
        in_specs=(
            P(("sp", "tp"), None),
            P(),
            P("sp", "tp"),
            P("sp", "tp"),
            P("sp", "tp"),
            P("sp", "tp"),
            P("sp", "tp"),
            P("sp", "tp"),
            P("sp", "tp"),
            P(),
            P(),
            P(),
            P("sp", "tp"),
            P("sp", "tp"),
        ),
        out_specs=P(("sp", "tp"), None),
        check_vma=False,
    )
```

profile of v0, /device:TPU:24, one launch (start us, length us, event | category | flops | bytes accessed | tf_op | source)
XLA Modules:
  0.0 722.7 jit_solution(9011163686985184079)
XLA Ops:
  6.5 1.2 fusion.15
  7.8 2.0 fusion.17
  9.9 0.7 all-gather.18.cloned.1.call-update
  13.3 1.8 multiply_cosine_fusion
  15.0 18.5 %all-gather.14.cloned.1.call-done = bf16[512,2048]{1,0:T(8,128)(2,1)} async-done(((bf16[128,2048]{1,0:T(8,128)(2,1)}), bf16[512,2048]{1,0:T(8,128)(2,1)}) %all-gather.14.cloned.1.call-update) | async-done | bytes 2097168 | tf_op jit(solution)/shard_map/all_gather | solution.py:182
  33.5 49.8 %all-gather.18.cloned.1.call-done = bf16[2048,512]{1,0:T(8,128)(2,1)} async-done(((bf16[256,512]{1,0:T(8,128)(2,1)}), bf16[2048,512]{1,0:T(8,128)(2,1)}) %all-gather.18.cloned.1.call-update) | async-done | bytes 2097168 | tf_op jit(solution)/shard_map/all_gather | solution.py:159
  83.3 3.5 convolution_convert_fusion.6
  87.4 45.7 %all-gather.20.cloned.1.call-done = bf16[2048,512]{1,0:T(8,128)(2,1)} async-done(((bf16[256,512]{1,0:T(8,128)(2,1)}), bf16[2048,512]{1,0:T(8,128)(2,1)}) %all-gather.20.cloned.1.call-update) | async-done | bytes 2097168 | tf_op jit(solution)/shard_map/all_gather | solution.py:160
  133.1 3.5 convolution_convert_fusion.5
  137.1 2.0 multiply_subtract_fusion
  139.2 67.3 %all-gather.16.cloned.1.call-done = bf16[2048,1024]{1,0:T(8,128)(2,1)} async-done(((bf16[256,1024]{1,0:T(8,128)(2,1)}), bf16[2048,1024]{1,0:T(8,128)(2,1)}) %all-gather.16.cloned.1.call-update) | async-done | bytes 4194320 | tf_op jit(solution)/shard_map/all_gather | solution.py:161
  206.4 5.2 convolution_convert_fusion.1
  211.6 1.6 fusion.24
  213.3 0.7 all-gather.22.cloned.1.call-update
  216.6 1.5 constant_dynamic-slice_fusion
  218.1 38.0 %all-gather.26.cloned.1.call-done = bf16[2048,512]{1,0:T(8,128)(2,1)} async-done(((bf16[256,512]{1,0:T(8,128)(2,1)}), bf16[2048,512]{1,0:T(8,128)(2,1)}) %all-gather.26.cloned.1.call-update) | async-done | bytes 2097168 | tf_op jit(solution)/shard_map/all_gather | solution.py:163
  256.0 4.4 fusion.14
  260.5 45.2 %all-gather.28.cloned.1.call-done = bf16[2048,512]{1,0:T(8,128)(2,1)} async-done(((bf16[256,512]{1,0:T(8,128)(2,1)}), bf16[2048,512]{1,0:T(8,128)(2,1)}) %all-gather.28.cloned.1.call-update) | async-done | bytes 2097168 | tf_op jit(solution)/shard_map/all_gather | solution.py:164
  305.7 3.9 fusion.13
  309.6 2.5 collective-permute-start
  312.1 1.8 fusion.89
  313.9 16.8 %all-gather.1 = f32[8,1,2]{2,1,0:T(1,128)} all-gather(f32[1,1,2]{2,1,0:T(1,128)S(1)} %exponential_bitcast_fusion), channel_id=1, replica_groups=mesh['sp'=8,'tp'=4] {'sp'}, dimensions={0}, use_global_device_ids=true | all-gather | bytes 72 | tf_op jit(solution)/shard_map/all_gather | solution.py:21
  330.7 1.3 dynamic_slice.20
  332.0 1.3 dynamic_slice.21
  333.3 5.4 fusion.86
  339.0 4.3 fusion.6
  343.3 87.1 %all-gather.34.cloned.1.call-done = f32[16,256,512]{2,1,0:T(8,128)} async-done(((f32[2,256,512]{2,1,0:T(8,128)}), f32[16,256,512]{2,1,0:T(8,128)}) %all-gather.34.cloned.1.call-update) | async-done | bytes 8388624 | tf_op jit(solution)/shard_map/all_gather | solution.py:21
  430.5 13.7 %while.12 = (s32[]{:T(128)}, f32[2,256,512]{2,1,0:T(8,128)S(1)}, s32[]{:T(128)}, f32[8,2]{1,0:T(8,128)}, f32[8,2,256,512]{3,2,1,0:T(8,128)}, /*index=5*/s32[]{:T(128)}, s32[]{:T(128)}, s32[]{:T(128)}) while((s32[]{:T(128)}, f32[2,256,512]{2,1,0:T(8,128)S(1)}, s32[]{:T(128)}, f32[8,2]{1,0:T(8,128)}, f32[8,2,256,512]{3,2,1,0:T(8,128)}, ...), condition=%wide.region_2.3_spmd, body=%wide.region_1.2_spmd.sunk | while | flops 524293 | bytes 3145879 | solution.py:29
  430.6 0.7 dynamic-slice_bitcast_fusion.2
  431.2 1.6 bitcast_add_fusion.2
  432.8 0.7 dynamic-slice_bitcast_fusion.2
  433.5 1.6 bitcast_add_fusion.2
  435.1 0.7 dynamic-slice_bitcast_fusion.2
  435.8 1.6 bitcast_add_fusion.2
  437.4 0.7 dynamic-slice_bitcast_fusion.2
  438.1 1.6 bitcast_add_fusion.2
  439.6 0.7 dynamic-slice_bitcast_fusion.2
  440.3 1.6 bitcast_add_fusion.2
  442.7 1.6 bitcast_add_fusion.2
  444.3 3.5 fusion.90
  448.4 1.9 copy.36
  450.3 53.8 %all-gather.22.cloned.1.call-done = bf16[2048,1024]{1,0:T(8,128)(2,1)} async-done(((bf16[256,1024]{1,0:T(8,128)(2,1)}), bf16[2048,1024]{1,0:T(8,128)(2,1)}) %all-gather.22.cloned.1.call-update) | async-done | bytes 4194320 | tf_op jit(solution)/shard_map/all_gather | solution.py:162
  504.0 73.5 %all-gather.24.cloned.1.call-done = bf16[2048,1024]{1,0:T(8,128)(2,1)} async-done(((bf16[256,1024]{1,0:T(8,128)(2,1)}), bf16[2048,1024]{1,0:T(8,128)(2,1)}) %all-gather.24.cloned.1.call-update) | async-done | bytes 4194320 | tf_op jit(solution)/shard_map/all_gather | solution.py:166
  577.5 11.4 %fusion.35 = f32[512,2048]{1,0:T(8,128)} fusion(bf16[2048,1024]{1,0:T(8,128)(2,1)} %all-gather.24.cloned.1.call-done, f32[512,1024]{1,0:T(8,128)} %copy.36, bf16[512,2048]{1,0:T(8,128)(2,1)} %all-gather.14.cloned.1.call-done, bf16[2048,1024]{1,0:T(8,128)(2,1)} %all-gather.22.cloned.1.call-done), kind=kOutput, calls=%fused_computation.89 | convolution fusion | flops 4299161600 | bytes 16777216 | tf_op jit(solution)/shard_map/dot_general | solution.py:128
  588.9 38.3 %all-gather.30.cloned.1.call-done = bf16[2048,512]{1,0:T(8,128)(2,1)} async-done(((bf16[256,512]{1,0:T(8,128)(2,1)}), bf16[2048,512]{1,0:T(8,128)(2,1)}) %all-gather.30.cloned.1.call-update) | async-done | bytes 2097168 | tf_op jit(solution)/shard_map/all_gather | solution.py:165
  627.1 49.8 %all-gather.32.cloned.1.call-done = bf16[2048,512]{1,0:T(8,128)(2,1)} async-done(((bf16[256,512]{1,0:T(8,128)(2,1)}), bf16[2048,512]{1,0:T(8,128)(2,1)}) %all-gather.32.cloned.1.call-update) | async-done | bytes 2097168 | tf_op jit(solution)/shard_map/all_gather | solution.py:167
  676.9 7.6 %add_convert_fusion = bf16[512,2048]{1,0:T(8,128)(2,1)} fusion(f32[512,2048]{1,0:T(8,128)} %fusion.35, bf16[2048,512]{1,0:T(8,128)(2,1)} %all-gather.32.cloned.1.call-done, bf16[512,2048]{1,0:T(8,128)(2,1)S(1)} %copy-done.5, bf16[2048,512]{1,0:T(8,128)(2,1)} %all-gather.30.cloned.1.call-done, f32[512,512]{1,0:T(8,128)S(1)} %get-tuple-element.71, ...), kind=kOutput, calls=%fused_computation.31 | convolution fusion | flops 2153775104 | bytes 13639680 | tf_op jit(solution)/shard_map/dot_general | solution.py:128
  684.5 31.3 %reduce-scatter.2.cloned.1.call-done = bf16[128,2048]{1,0:T(8,128)(2,1)} async-done(((bf16[512,2048]{1,0:T(8,128)(2,1)}), bf16[128,2048]{1,0:T(8,128)(2,1)}) %reduce-scatter.2.cloned.1.call-update) | async-done | bytes 524304 | tf_op jit(solution)/shard_map/reduce_scatter | solution.py:217
  (62 shorter events, 7.9 us)
Async XLA Ops:
  6.5 27.0 %all-gather.14.cloned.1.call-start = ((), (), s32[]{:S(2)}) async-start(), calls=%async_computation.1 | async-start | bytes 2621440 | tf_op jit(solution)/shard_map/all_gather | solution.py:182
  9.8 73.5 %all-gather.18.cloned.1.call-start = ((), (), s32[]{:S(2)}) async-start(), calls=%async_computation.3 | async-start | bytes 2359296 | tf_op jit(solution)/shard_map/all_gather | solution.py:159
  10.6 122.5 %all-gather.20.cloned.1.call-start = ((), (), s32[]{:S(2)}) async-start(), calls=%async_computation.4 | async-start | bytes 2359296 | tf_op jit(solution)/shard_map/all_gather | solution.py:160
  11.3 195.1 %all-gather.16.cloned.1.call-start = ((), (), s32[]{:S(2)}) async-start(), calls=%async_computation.2 | async-start | bytes 4718592 | tf_op jit(solution)/shard_map/all_gather | solution.py:161
  11.9 244.2 %all-gather.26.cloned.1.call-start = ((), (), s32[]{:S(2)}) async-start(), calls=%async_computation.7 | async-start | bytes 2359296 | tf_op jit(solution)/shard_map/all_gather | solution.py:163
  12.5 293.2 %all-gather.28.cloned.1.call-start = ((), (), s32[]{:S(2)}) async-start(), calls=%async_computation.8 | async-start | bytes 2359296 | tf_op jit(solution)/shard_map/all_gather | solution.py:164
  13.1 417.4 %all-gather.34.cloned.1.call-start = ((), (), s32[]{:S(2)}) async-start(), calls=%async_computation.12 | async-start | bytes 9437184 | tf_op jit(solution)/shard_map/all_gather | solution.py:21
  13.1 73.7 %copy-start.4 = (f32[2]{0:T(128)}, f32[2]{0:T(128)S(1)}, u32[]{:S(2)}) copy-start(f32[2]{0:T(128)S(1)} %add_multiply_fusion) | copy-start | bytes 28
  139.1 72.4 %copy-start = (f32[512,2,128]{2,0,1:T(8,128)}, f32[512,2,128]{2,0,1:T(8,128)S(1)}, u32[]{:S(2)}) copy-start(f32[512,2,128]{2,0,1:T(8,128)S(1)} %get-tuple-element.72) | copy-start | bytes 1572868
  139.2 72.4 %copy-start.1 = (f32[512,2,128]{2,0,1:T(8,128)S(1)}, f32[512,2,128]{2,0,1:T(8,128)}, u32[]{:S(2)}) copy-start(f32[512,2,128]{2,0,1:T(8,128)} %get-tuple-element.73) | copy-start | bytes 1572868
  211.6 1.7 copy-start.6
  213.3 290.7 %all-gather.22.cloned.1.call-start = ((), (), s32[]{:S(2)}) async-start(), calls=%async_computation.5 | async-start | bytes 4718592 | tf_op jit(solution)/shard_map/all_gather | solution.py:162
  214.0 363.5 %all-gather.24.cloned.1.call-start = ((), (), s32[]{:S(2)}) async-start(), calls=%async_computation.6 | async-start | bytes 4718592 | tf_op jit(solution)/shard_map/all_gather | solution.py:166
  214.8 412.4 %all-gather.30.cloned.1.call-start = ((), (), s32[]{:S(2)}) async-start(), calls=%async_computation.9 | async-start | bytes 2359296 | tf_op jit(solution)/shard_map/all_gather | solution.py:165
  215.3 461.6 %all-gather.32.cloned.1.call-start = ((), (), s32[]{:S(2)}) async-start(), calls=%async_computation.10 | async-start | bytes 2359296 | tf_op jit(solution)/shard_map/all_gather | solution.py:167
  216.1 499.7 %reduce-scatter.2.cloned.1.call-start = ((), (), s32[]{:S(2)}) async-start(), calls=%async_computation.11 | async-start | bytes 2621440 | tf_op jit(solution)/shard_map/reduce_scatter | solution.py:217
  309.6 23.8 %collective-permute-start = (bf16[30,512]{1,0:T(8,128)(2,1)S(1)}, bf16[30,512]{1,0:T(8,128)(2,1)S(1)}, u32[]{:S(2)}, u32[]{:S(2)}) collective-permute-start(bf16[30,512]{1,0:T(8,128)(2,1)S(1)} %slice.268), channel_id=1, source_target_pairs={{0,4},{4,8},{8,12},{12,16},{16,20},{20,24},{24,28},{1,5},{5,9},{9,... | collective-permute-start | bytes 92168 | tf_op jit(solution)/shard_map/ppermute | solution.py:35
  450.2 226.7 %copy-start.2 = (f32[512]{0:T(512)S(1)}, f32[512]{0:T(512)}, u32[]{:S(2)}) copy-start(f32[512]{0:T(512)} %dynamic_slice.20) | copy-start | bytes 6148
  450.3 226.7 %copy-start.3 = (f32[512]{0:T(512)S(1)}, f32[512]{0:T(512)}, u32[]{:S(2)}) copy-start(f32[512]{0:T(512)} %dynamic_slice.21) | copy-start | bytes 6148
  450.3 226.7 %copy-start.5 = (bf16[512,2048]{1,0:T(8,128)(2,1)S(1)}, bf16[512,2048]{1,0:T(8,128)(2,1)}, u32[]{:S(2)}) copy-start(bf16[512,2048]{1,0:T(8,128)(2,1)} %all-gather.14.cloned.1.call-done) | copy-start | bytes 6291460
Sparse Core Ops, SparseCore 0:
  9.9 23.5 all-gather.13
  35.6 47.6 all-gather.17
  85.4 47.6 all-gather.19
  135.1 71.3 all-gather.15
  208.4 47.6 all-gather.25
  258.0 47.6 all-gather.27
  307.8 122.5 all-gather.33
  432.5 71.4 all-gather.21
  506.1 71.3 all-gather.23
  579.5 47.6 all-gather.29
  629.3 47.6 all-gather.31
  684.6 31.1 reduce-scatter.1
where the time goes:
time: 725 us; the launch traced here: 723 us
  waiting for transfers between devices  604 us (83%)
  matrix products  48.9 us (7%)
  other arithmetic  23.2 us (3%)
  blocking collectives  16.8 us (2%)
  between operations  13.8 us (2%)
  local copies, waits for them, and re-layouts  13.1 us (2%)
    all_gather x1, waiting for transfers between devices, carried_in(): gathered = jax.tree.map(lambda a: lax.all_gather(a, axis), part)  87.1 us
    all_gather x1, waiting for transfers between devices, local(): lax.all_gather(retain_output, 'sp', axis=0, tiled=True)  73.5 us
    all_gather x1, waiting for transfers between devices, local(): lax.all_gather(value_weight, 'sp', axis=0, tiled=True)  67.3 us
    all_gather x1, waiting for transfers between devices, local(): lax.all_gather(retain_gate, 'sp', axis=0, tiled=True)  53.8 us
    all_gather x1, waiting for transfers between devices, local(): lax.all_gather(convolve_output, 'sp', axis=0, tiled=True)  49.8 us
    all_gather x1, waiting for transfers between devices, local(): lax.all_gather(query_weight, 'sp', axis=0, tiled=True)  49.8 us
    all_gather x1, waiting for transfers between devices, local(): lax.all_gather(key_weight, 'sp', axis=0, tiled=True)  45.7 us
    all_gather x1, waiting for transfers between devices, local(): lax.all_gather(unit_gate, 'sp', axis=0, tiled=True)  45.2 us
  transfers between devices with their start and end apart: 13, of which 12 were waited for; matrix products, arithmetic and copies ran while one was open for 10% of the time, Pallas kernels for 0%

commit v1 on v0

--- a/solution.py
+++ b/solution.py
@@ -13,26 +13,68 @@
 group_eps = 1.0
 layer_eps = 0.001
 rope_base = 10000.0
-highest = lax.Precision.HIGHEST
-
-
-def carried_in(part, axis, combine, identity):
-    place = lax.axis_index(axis)
-    gathered = jax.tree.map(lambda a: lax.all_gather(a, axis), part)
-    state = jax.tree.map(lambda a, e: jnp.zeros_like(a) + jnp.asarray(e, a.dtype), part, identity)
-
-    def one(hop, state):
-        return combine(
-            state, jax.tree.map(lambda a: lax.dynamic_index_in_dim(a, hop, 0, False), gathered)
-        )
-
-    return lax.fori_loop(0, place, one, state)
 
 
 def from_behind(x, axis, by):
     length = lax.axis_size(axis)
     pairs = [(i, i + by) for i in range(length) if 0 <= i + by < length]
     return lax.ppermute(x, axis, pairs)
+
+
+def partners(axis, bit):
+    return [(i, i ^ bit) for i in range(lax.axis_size(axis))]
+
+
+def gather_rows(x, axis):
+    rank = lax.axis_index(axis)
+    blocks = x[None]
+    bit = lax.axis_size(axis) // 2
+    while bit >= 1:
+        other = lax.ppermute(blocks, axis, partners(axis, bit))
+        low = (rank & bit) == 0
+        blocks = jnp.stack(
+            [jnp.where(low, blocks, other), jnp.where(low, other, blocks)], axis=1
+        ).reshape((-1,) + x.shape)
+        bit //= 2
+    return blocks.reshape((-1,) + x.shape[1:])
+
+
+def scatter_sums(make, hidden, axis):
+    size = lax.axis_size(axis)
+    rank = lax.axis_index(axis)
+    rows = hidden.shape[0] // size
+    parity = rank & 1
+    paired = hidden.reshape(size // 2, 2, rows, hidden.shape[1])
+
+    def half(which):
+        taken = lax.dynamic_index_in_dim(paired, which, 1, False)
+        return make(taken.reshape(-1, hidden.shape[1])).reshape(size // 2, rows, -1)
+
+    away = half(1 - parity).astype(jnp.bfloat16)
+    arrived = lax.ppermute(away, axis, partners(axis, 1))
+    total = half(parity) + arrived.astype(jnp.float32)
+    bit = 2
+    while bit < size:
+        mine = (rank // bit) & 1
+        split = total.reshape(-1, 2, rows, total.shape[-1])
+        away = lax.dynamic_index_in_dim(split, 1 - mine, 1, False).astype(jnp.bfloat16)
+        arrived = lax.ppermute(away, axis, partners(axis, bit))
+        total = lax.dynamic_index_in_dim(split, mine, 1, False) + arrived.astype(jnp.float32)
+        bit *= 2
+    return total.reshape(rows, -1).astype(jnp.bfloat16)
+
+
+def state_before(contribution, totals, axis):
+    size = lax.axis_size(axis)
+    carried = from_behind(contribution.astype(jnp.bfloat16), axis, 1).astype(jnp.float32)
+    decay = totals
+    reach = 1
+    while reach < size - 1:
+        earlier = from_behind(carried.astype(jnp.bfloat16), axis, reach).astype(jnp.float32)
+        carried = carried + decay[:, None, None] * earlier
+        decay = decay * decay
+        reach *= 2
+    return carried
 
 
 def rms_normalize(tokens, norm_gain):
@@ -95,7 +137,12 @@
     indices = jnp.arange(row_count, dtype=jnp.float32)
     leading = jnp.exp(log_decay[None, :] * (indices + 1.0)[:, None])
     return (
-        jnp.einsum("ihd,hde->ihe", queries.astype(jnp.float32), carry_state, precision=highest)
+        jnp.einsum(
+            "ihd,hde->ihe",
+            queries,
+            carry_state.astype(jnp.bfloat16),
+            preferred_element_type=jnp.float32,
+        )
         * leading[:, :, None]
     )
 
@@ -128,10 +175,6 @@
     return lax.dot_general(
         hidden, matrix, (((1,), (1,)), ((), ())), preferred_element_type=jnp.float32
     )
-
-
-def join_states(earlier, later):
-    return (earlier[0] * later[0], later[0][:, None, None] * earlier[1] + later[1])
 
 
 def local(
@@ -155,32 +198,22 @@
     head_rank = lax.axis_index("tp")
     chain_rank = lax.axis_index("sp")
     normed = rms_normalize(tokens, norm_gain)
-    gathered = (
-        lax.all_gather(query_weight, "sp", axis=0, tiled=True),
-        lax.all_gather(key_weight, "sp", axis=0, tiled=True),
-        lax.all_gather(value_weight, "sp", axis=0, tiled=True),
-        lax.all_gather(retain_gate, "sp", axis=0, tiled=True),
-        lax.all_gather(unit_value, "sp", axis=0, tiled=True),
-        lax.all_gather(unit_gate, "sp", axis=0, tiled=True),
-        lax.all_gather(convolve_gate, "sp", axis=0, tiled=True),
-        lax.all_gather(retain_output, "sp", axis=0, tiled=True),
-        lax.all_gather(convolve_output, "sp", axis=0, tiled=True),
-    )
-    in_weights = gathered[:7]
-    retain_full = gathered[7]
-    convolve_full = gathered[8]
-
-    def project(row_piece):
-        return jnp.concatenate(
-            [
-                jnp.dot(row_piece, matrix, preferred_element_type=jnp.float32).astype(jnp.bfloat16)
-                for matrix in in_weights
-            ],
-            axis=1,
-        )
-
-    projected = project(lax.all_gather(normed, "tp", axis=0, tiled=True))
-    row_count = projected.shape[0]
+    in_weights = (
+        query_weight,
+        key_weight,
+        value_weight,
+        retain_gate,
+        unit_value,
+        unit_gate,
+        convolve_gate,
+    )
+    in_full = lax.all_gather(jnp.concatenate(in_weights, axis=1), "sp", axis=0, tiled=True)
+    out_full = lax.all_gather(
+        jnp.concatenate((retain_output, convolve_output), axis=1), "sp", axis=0, tiled=True
+    )
+    rows = gather_rows(normed, "tp")
+    row_count = rows.shape[0]
+    projected = jnp.dot(rows, in_full, preferred_element_type=jnp.float32).astype(jnp.bfloat16)
     bounds = [0]
     for matrix in in_weights:
         bounds.append(bounds[-1] + matrix.shape[1])
@@ -199,13 +232,7 @@
     ).astype(jnp.bfloat16)
     channels = gated_input.shape[1]
     before = from_behind(gated_input[row_count - (KW - 1) :], "sp", 1)
-    prefix = carried_in(
-        (totals, contribution),
-        "sp",
-        join_states,
-        (jnp.ones_like(totals), jnp.zeros_like(contribution)),
-    )
-    incoming = prefix[1]
+    incoming = state_before(contribution, totals, "sp")
     raw = within + cross_part(rotated_query, incoming, log_decay)
     retain_hidden = retain_finish(raw, retain_switch)
     tap_slice = lax.dynamic_slice_in_dim(filter_taps, head_rank * channels, channels, 1)
@@ -214,14 +241,8 @@
     convolve_hidden = convolve_branch(
         gated_input, before, tap_slice, gain_slice, shift_slice, convolve_switch
     )
-    return lax.psum_scatter(
-        (contract(retain_hidden, retain_full) + contract(convolve_hidden, convolve_full)).astype(
-            jnp.bfloat16
-        ),
-        "tp",
-        scatter_dimension=0,
-        tiled=True,
-    )
+    hidden = jnp.concatenate((retain_hidden, convolve_hidden), axis=1)
+    return scatter_sums(lambda rows: contract(rows, out_full), hidden, "tp")
 
 
 def solution(mesh):

time: 725 us -> 571 us (0.79)
  waiting for transfers between devices: 604 us -> 464 us
  matrix products: 48.9 us -> 31.2 us
  blocking collectives: 16.8 us -> 0 us
  starting transfers between devices: 2.89 us -> 12.1 us
    all_gather x11 -> x2, waiting for transfers between devices: 567 us -> 344 us  [the longest x1 344 us: local(): lax.all_gather(jnp.concatenate(in_weights, axis=1), 'sp', axis=0, tiled=T...]
    ppermute x1 -> x5, waiting for transfers between devices: 0.01 us -> 94.3 us  [from_behind(): return lax.ppermute(x, axis, pairs)]
    reduce_scatter x1 -> x0, waiting for transfers between devices: 31.3 us -> none  [local(): lax.psum_scatter((contract(retain_hidden, retain_full) + contract(convolv...]
    ppermute x0 -> x4, waiting for transfers between devices: none -> 25.6 us  [the longest x1 12.5 us: scatter_sums(): arrived = lax.ppermute(away, axis, partners(axis, bit))]
    all_gather x1 -> x0, blocking collectives: 16.8 us -> none  [carried_in(): gathered = jax.tree.map(lambda a: lax.all_gather(a, axis), part)]
    add x6 -> x0, other arithmetic: 9.41 us -> none  [join_states(): later[0][:, None, None] * earlier[1] + later[1]]
    dot_general x6 -> x2, matrix products: 24 us -> 14.7 us  [the longest x1 13.8 us: local(): jnp.dot(rows, in_full, preferred_element_type=jnp.float32)]
    dot_general x2, matrix products: 18.9 us -> 11.6 us  [contract(): lax.dot_general(hidden, matrix, (((1,), (1,)), ((), ())), preferred_eleme...]
  transfers between devices with their start and end apart: 13 -> 11, of which waited for: 12 -> 8; matrix products, arithmetic and copies ran while one was open for 10% -> 10% of each run, Pallas kernels for 0% -> 0%
where the time goes in v1:
time: 571 us; the launch traced here: 566 us
  waiting for transfers between devices  464 us (81%)
  matrix products  31.2 us (5%)
  other arithmetic  25.3 us (4%)
  local copies, waits for them, and re-layouts  19 us (3%)
  between operations  13.9 us (2%)
  starting transfers between devices  12.1 us (2%)
    all_gather x1, waiting for transfers between devices, local(): lax.all_gather(jnp.concatenate(in_weights, axis=1), 'sp', axis=0, tiled=T...  344 us
    ppermute x5, waiting for transfers between devices, from_behind(): return lax.ppermute(x, axis, pairs)  94.3 us
    dot_general x1, matrix products, local(): jnp.dot(rows, in_full, preferred_element_type=jnp.float32)  13.8 us
    ppermute x1, waiting for transfers between devices, scatter_sums(): arrived = lax.ppermute(away, axis, partners(axis, bit))  12.5 us
    dot_general x2, matrix products, contract(): lax.dot_general(hidden, matrix, (((1,), (1,)), ((), ())), preferred_eleme...  11.6 us
  transfers between devices with their start and end apart: 11, of which 8 were waited for; matrix products, arithmetic and copies ran while one was open for 10% of the time, Pallas kernels for 0%

profile of v1, /device:TPU:24, one launch (start us, length us, event | category | flops | bytes accessed | tf_op | source)
XLA Modules:
  0.0 565.9 jit_solution(14118452360818894991)
XLA Ops:
  6.5 1.1 constant_dynamic-update-slice_fusion.6
  7.6 1.0 constant_dynamic-update-slice_fusion.5
  8.6 1.1 constant_dynamic-update-slice_fusion.4
  9.9 1.4 copy-done.2
  11.8 1.6 collective-permute-start
  13.4 1.9 pad_maximum_fusion.2
  15.3 10.2 %collective-permute-done = bf16[1,128,2048]{2,1,0:T(8,128)(2,1)S(1)} collective-permute-done((bf16[1,128,2048]{2,1,0:T(8,128)(2,1)S(1)}, bf16[1,128,2048]{2,1,0:T(8,128)(2,1)S(1)}, u32[]{:S(2)}, u32[]{:S(2)}) %collective-permute-start) | collective-permute-done | bytes 524320 | tf_op jit(solution)/shard_map/ppermute | solution.py:33
  25.9 1.1 maximum_bitcast_fusion
  27.7 0.6 fusion.93
  28.3 1.7 multiply_cosine_fusion
  30.4 344.5 %all-gather.3.cloned.1.call-done = bf16[2048,4608]{1,0:T(8,128)(2,1)} async-done(((bf16[256,4608]{1,0:T(8,128)(2,1)}), bf16[2048,4608]{1,0:T(8,128)(2,1)}) %all-gather.3.cloned.1.call-update) | async-done | bytes 18874384 | tf_op jit(solution)/shard_map/all_gather | solution.py:210
  374.8 13.8 %convolution_convert_fusion = bf16[512,4608]{1,0:T(8,128)(2,1)S(1)} fusion(bf16[512,2048]{1,0:T(8,128)(2,1)S(1)} %bitcast.88, bf16[2048,4608]{1,0:T(8,128)(2,1)} %all-gather.3.cloned.1.call-done), kind=kOutput, calls=%fused_computation | convolution fusion | flops 9666035712 | bytes 25690112 | tf_op jit(solution)/shard_map/dot_general | solution.py:216
  388.6 1.2 slice.292
  390.2 0.9 copy-done
  391.1 0.7 reshape.274
  391.8 0.7 reshape.276
  392.5 0.7 fusion.96
  393.7 0.8 copy-done.8
  394.6 0.7 convolution_convert_fusion.1
  395.3 2.3 collective-permute-start.2
  398.2 1.3 dynamic_slice.20
  399.6 1.4 dynamic_slice.21
  400.9 1.1 fusion.98
  402.0 2.0 constant_dynamic-slice_fusion
  404.3 1.2 fusion.27
  405.5 19.3 %collective-permute-done.2 = bf16[2,256,512]{2,1,0:T(8,128)(2,1)S(1)} collective-permute-done((bf16[2,256,512]{2,1,0:T(8,128)(2,1)S(1)}, bf16[2,256,512]{2,1,0:T(8,128)(2,1)S(1)}, u32[]{:S(2)}, u32[]{:S(2)}) %collective-permute-start.2) | collective-permute-done | bytes 524320 | tf_op jit(solution)/shard_map/ppermute | solution.py:21
  424.8 1.9 collective-permute-start.3
  426.7 1.5 multiply_convert_fusion.1
  428.3 2.1 collective-permute-start.6
  430.4 4.3 fusion.13
  434.7 28.5 %collective-permute-done.3 = bf16[2,256,512]{2,1,0:T(8,128)(2,1)S(1)} collective-permute-done((bf16[2,256,512]{2,1,0:T(8,128)(2,1)S(1)}, bf16[2,256,512]{2,1,0:T(8,128)(2,1)S(1)}, u32[]{:S(2)}, u32[]{:S(2)}) %collective-permute-start.3) | collective-permute-done | bytes 524320 | tf_op jit(solution)/shard_map/ppermute | solution.py:21
  463.2 0.9 fusion.31
  464.1 1.3 collective-permute-start.4
  465.4 5.6 fusion.95
  471.3 21.7 %collective-permute-done.4 = bf16[2,256,512]{2,1,0:T(8,128)(2,1)S(1)} collective-permute-done((bf16[2,256,512]{2,1,0:T(8,128)(2,1)S(1)}, bf16[2,256,512]{2,1,0:T(8,128)(2,1)S(1)}, u32[]{:S(2)}, u32[]{:S(2)}) %collective-permute-start.4) | collective-permute-done | bytes 524320 | tf_op jit(solution)/shard_map/ppermute | solution.py:21
  493.4 1.3 collective-permute-start.5
  494.7 1.7 fusion.29
  496.4 24.7 %collective-permute-done.5 = bf16[2,256,512]{2,1,0:T(8,128)(2,1)S(1)} collective-permute-done((bf16[2,256,512]{2,1,0:T(8,128)(2,1)S(1)}, bf16[2,256,512]{2,1,0:T(8,128)(2,1)S(1)}, u32[]{:S(2)}, u32[]{:S(2)}) %collective-permute-start.5) | collective-permute-done | bytes 524320 | tf_op jit(solution)/shard_map/ppermute | solution.py:21
  521.1 0.9 fusion.99
  522.6 1.9 copy.36
  524.4 2.5 fusion.12
  527.1 5.6 fusion.4
  532.7 2.9 collective-permute-done.7
  535.6 6.0 %convert_add_fusion = f32[2,128,2048]{2,1,0:T(8,128)} fusion(bf16[2,128,2048]{2,1,0:T(8,128)(2,1)S(1)} %collective-permute-done.7, bf16[2048,1536]{1,0:T(8,128)(2,1)} %all-gather.5.cloned.1.call-done, bf16[2,2,128,1536]{3,2,1,0:T(8,128)(2,1)S(1)} %bitcast.90, s32[]{:T(128)S(6)} %select_n.69), kind=kOutput, calls=%fused_computation.44 | convolution fusion | flops 1611661312 | bytes 10223620 | tf_op jit(solution)/shard_map/dot_general | solution.py:175
  541.6 1.3 dynamic-slice_convert_fusion
  542.9 1.5 collective-permute-start.8
  544.4 12.5 %collective-permute-done.8 = bf16[1,128,2048]{2,1,0:T(8,128)(2,1)S(1)} collective-permute-done((bf16[1,128,2048]{2,1,0:T(8,128)(2,1)S(1)}, bf16[1,128,2048]{2,1,0:T(8,128)(2,1)S(1)}, u32[]{:S(2)}, u32[]{:S(2)}) %collective-permute-start.8) | collective-permute-done | bytes 524320 | tf_op jit(solution)/shard_map/ppermute | solution.py:61
  556.9 2.1 fusion.43
  (76 shorter events, 5.0 us)
Async XLA Ops:
  6.5 3.1 copy-start.7
  6.5 3.2 copy-start.10
  6.5 3.2 copy-start.11
  6.5 368.3 %all-gather.3.cloned.1.call-start = ((), (), s32[]{:S(2)}) async-start(), calls=%async_computation | async-start | bytes 21233664 | tf_op jit(solution)/shard_map/all_gather | solution.py:210
  6.5 3.3 copy-start.12
  9.7 1.7 copy-start.1
  9.8 1.8 copy-start.13
  9.9 1.4 copy-start.2
  9.9 3.5 copy-start.6
  11.3 515.8 %all-gather.5.cloned.1.call-start = ((), (), s32[]{:S(2)}) async-start(), calls=%async_computation.1 | async-start | bytes 7077888 | tf_op jit(solution)/shard_map/all_gather | solution.py:211
  11.8 13.7 %collective-permute-start = (bf16[1,128,2048]{2,1,0:T(8,128)(2,1)S(1)}, bf16[1,128,2048]{2,1,0:T(8,128)(2,1)S(1)}, u32[]{:S(2)}, u32[]{:S(2)}) collective-permute-start(bf16[1,128,2048]{2,1,0:T(8,128)(2,1)S(1)} %fusion.44), channel_id=1, source_target_pairs={{0,2},{1,3},{2,0},{3,1},{4,6},{5,7},{6,4},{7,5},{8,10},{9,11},{10,... | collective-permute-start | bytes 1572872 | tf_op jit(solution)/shard_map/ppermute | solution.py:33
  27.0 3.0 collective-permute-start.1
  27.0 3.1 copy-start.19
  388.6 2.5 copy-start
  392.4 1.0 copy-start.4
  393.4 1.2 copy-start.5
  393.7 0.9 copy-start.8
  393.7 1.6 copy-start.9
  395.3 29.5 %collective-permute-start.2 = (bf16[2,256,512]{2,1,0:T(8,128)(2,1)S(1)}, bf16[2,256,512]{2,1,0:T(8,128)(2,1)S(1)}, u32[]{:S(2)}, u32[]{:S(2)}) collective-permute-start(bf16[2,256,512]{2,1,0:T(8,128)(2,1)S(1)} %convolution_convert_fusion.1), channel_id=1, source_target_pairs={{0,4},{4,8},{8,12},{12,16},{16,20},{20,24},{24,28},{1,5},{5,9},{9,... | collective-permute-start | bytes 1572872 | tf_op jit(solution)/shard_map/ppermute | solution.py:21
  424.8 38.4 %collective-permute-start.3 = (bf16[2,256,512]{2,1,0:T(8,128)(2,1)S(1)}, bf16[2,256,512]{2,1,0:T(8,128)(2,1)S(1)}, u32[]{:S(2)}, u32[]{:S(2)}) collective-permute-start(bf16[2,256,512]{2,1,0:T(8,128)(2,1)S(1)} %collective-permute-done.2), channel_id=1, source_target_pairs={{0,4},{4,8},{8,12},{12,16},{16,20},{20,24},{24,28},{1,5},{5,9},{9,... | collective-permute-start | bytes 1572872 | tf_op jit(solution)/shard_map/ppermute | solution.py:21
  428.3 37.2 %collective-permute-start.6 = (bf16[30,512]{1,0:T(8,128)(2,1)S(1)}, bf16[30,512]{1,0:T(8,128)(2,1)S(1)}, u32[]{:S(2)}, u32[]{:S(2)}) collective-permute-start(bf16[30,512]{1,0:T(8,128)(2,1)S(1)} %slice.302), channel_id=1, source_target_pairs={{0,4},{4,8},{8,12},{12,16},{16,20},{20,24},{24,28},{1,5},{5,9},{9,... | collective-permute-start | bytes 92168 | tf_op jit(solution)/shard_map/ppermute | solution.py:21
  434.7 58.4 %copy-start.16 = (f32[2]{0:T(128)S(1)}, f32[2]{0:T(128)}, u32[]{:S(2)}) copy-start(f32[2]{0:T(128)} %multiply_exponential_fusion.2) | copy-start | bytes 28
  434.7 58.4 %copy-start.17 = (f32[2]{0:T(128)S(1)}, f32[2]{0:T(128)}, u32[]{:S(2)}) copy-start(f32[2]{0:T(128)} %fusion.93) | copy-start | bytes 28
  464.1 29.0 %collective-permute-start.4 = (bf16[2,256,512]{2,1,0:T(8,128)(2,1)S(1)}, bf16[2,256,512]{2,1,0:T(8,128)(2,1)S(1)}, u32[]{:S(2)}, u32[]{:S(2)}) collective-permute-start(bf16[2,256,512]{2,1,0:T(8,128)(2,1)S(1)} %fusion.31), channel_id=1, source_target_pairs={{0,8},{4,12},{8,16},{12,20},{16,24},{20,28},{1,9},{5,13},{9,17},{1... | collective-permute-start | bytes 1572872 | tf_op jit(solution)/shard_map/ppermute | solution.py:21
  465.4 29.3 %copy-start.14 = (f32[512]{0:T(512)S(1)}, f32[512]{0:T(512)}, u32[]{:S(2)}) copy-start(f32[512]{0:T(512)} %dynamic_slice.20) | copy-start | bytes 6148
  465.4 29.3 %copy-start.15 = (f32[512]{0:T(512)S(1)}, f32[512]{0:T(512)}, u32[]{:S(2)}) copy-start(f32[512]{0:T(512)} %dynamic_slice.21) | copy-start | bytes 6148
  471.3 49.8 %copy-start.3 = (f32[2,512,512]{2,1,0:T(8,128)S(1)}, f32[2,512,512]{2,1,0:T(8,128)}, u32[]{:S(2)}) copy-start(f32[2,512,512]{2,1,0:T(8,128)} %fusion.13) | copy-start | bytes 6291460
  471.3 49.8 %copy-start.18 = (f32[2]{0:T(128)S(1)}, f32[2]{0:T(128)}, u32[]{:S(2)}) copy-start(f32[2]{0:T(128)} %fusion.94) | copy-start | bytes 28
  493.4 27.7 %collective-permute-start.5 = (bf16[2,256,512]{2,1,0:T(8,128)(2,1)S(1)}, bf16[2,256,512]{2,1,0:T(8,128)(2,1)S(1)}, u32[]{:S(2)}, u32[]{:S(2)}) collective-permute-start(bf16[2,256,512]{2,1,0:T(8,128)(2,1)S(1)} %fusion.42), channel_id=1, source_target_pairs={{0,16},{4,20},{8,24},{12,28},{1,17},{5,21},{9,25},{13,29},{2,18},{... | collective-permute-start | bytes 1572872 | tf_op jit(solution)/shard_map/ppermute | solution.py:21
  532.7 2.9 collective-permute-start.7
  542.9 14.0 %collective-permute-start.8 = (bf16[1,128,2048]{2,1,0:T(8,128)(2,1)S(1)}, bf16[1,128,2048]{2,1,0:T(8,128)(2,1)S(1)}, u32[]{:S(2)}, u32[]{:S(2)}) collective-permute-start(bf16[1,128,2048]{2,1,0:T(8,128)(2,1)S(1)} %dynamic-slice_convert_fusion), channel_id=1, source_target_pairs={{0,2},{1,3},{2,0},{3,1},{4,6},{5,7},{6,4},{7,5},{8,10},{9,11},{10,... | collective-permute-start | bytes 1572872 | tf_op jit(solution)/shard_map/ppermute | solution.py:61
Sparse Core Ops, SparseCore 0:
  11.5 363.3 all-gather.2
  377.0 122.4 all-gather.4

commit v2 on v1

--- a/solution.py
+++ b/solution.py
@@ -207,17 +207,29 @@
         unit_gate,
         convolve_gate,
     )
-    in_full = lax.all_gather(jnp.concatenate(in_weights, axis=1), "sp", axis=0, tiled=True)
-    out_full = lax.all_gather(
-        jnp.concatenate((retain_output, convolve_output), axis=1), "sp", axis=0, tiled=True
-    )
+    def whole(*parts):
+        packed = jnp.concatenate(parts, axis=1)
+        return lax.all_gather(packed, "sp", axis=0, tiled=True)
+
+    first = whole(*in_weights[:3])
+    second = whole(*in_weights[3:6])
+    third = whole(in_weights[6], retain_output, convolve_output)
+    width = convolve_gate.shape[1]
+    out_full = third[:, width:]
     rows = gather_rows(normed, "tp")
     row_count = rows.shape[0]
-    projected = jnp.dot(rows, in_full, preferred_element_type=jnp.float32).astype(jnp.bfloat16)
-    bounds = [0]
-    for matrix in in_weights:
-        bounds.append(bounds[-1] + matrix.shape[1])
-    pieces = [projected[:, bounds[column] : bounds[column + 1]] for column in range(7)]
+
+    def project(matrix, widths):
+        made = jnp.dot(rows, matrix, preferred_element_type=jnp.float32).astype(jnp.bfloat16)
+        bounds = [sum(widths[:i]) for i in range(len(widths) + 1)]
+        return [made[:, bounds[i] : bounds[i + 1]] for i in range(len(widths))]
+
+    widths = [matrix.shape[1] for matrix in in_weights]
+    pieces = (
+        project(first, widths[:3])
+        + project(second, widths[3:6])
+        + project(third[:, :width], widths[6:])
+    )
     queries, key_rows, values, retain_switch, glu_value, glu_switch, convolve_switch = pieces
     local_heads = queries.shape[1] // KEY
     positions = chain_rank * row_count + jnp.arange(row_count, dtype=jnp.int32)

time: 571 us -> 482 us (0.84)
  waiting for transfers between devices: 464 us -> 375 us
  matrix products: 31.2 us -> 39.1 us
    all_gather x2 -> x3, waiting for transfers between devices: 344 us -> 289 us  [whole(): return lax.all_gather(packed, 'sp', axis=0, tiled=True)]
    ppermute x5, waiting for transfers between devices: 94.3 us -> 61.9 us  [from_behind(): return lax.ppermute(x, axis, pairs)]
    dot_general x1 -> x3, matrix products: 13.8 us -> 20.9 us  [project(): jnp.dot(rows, matrix, preferred_element_type=jnp.float32)]
  transfers between devices with their start and end apart: 11 -> 12, of which waited for: 8 -> 8; matrix products, arithmetic and copies ran while one was open for 10% -> 11% of each run, Pallas kernels for 0% -> 0%
where the time goes in v2:
time: 482 us; the launch traced here: 481 us
  waiting for transfers between devices  375 us (78%)
  matrix products  39.1 us (8%)
  other arithmetic  25.6 us (5%)
  local copies, waits for them, and re-layouts  15.2 us (3%)
  between operations  13.6 us (3%)
  starting transfers between devices  13 us (3%)
    all_gather x3, waiting for transfers between devices, whole(): return lax.all_gather(packed, 'sp', axis=0, tiled=True)  289 us
    ppermute x5, waiting for transfers between devices, from_behind(): return lax.ppermute(x, axis, pairs)  61.9 us
    dot_general x3, matrix products, project(): jnp.dot(rows, matrix, preferred_element_type=jnp.float32)  20.9 us
    ppermute x1, waiting for transfers between devices, scatter_sums(): arrived = lax.ppermute(away, axis, partners(axis, bit))  12.5 us
    dot_general x2, matrix products, contract(): lax.dot_general(hidden, matrix, (((1,), (1,)), ((), ())), preferred_eleme...  10.2 us
    ppermute x5, starting transfers between devices, from_behind(): return lax.ppermute(x, axis, pairs)  9.72 us
  transfers between devices with their start and end apart: 12, of which 8 were waited for; matrix products, arithmetic and copies ran while one was open for 11% of the time, Pallas kernels for 0%

profile of v2, /device:TPU:24, one launch (start us, length us, event | category | flops | bytes accessed | tf_op | source)
XLA Modules:
  0.0 481.0 jit_solution(12745750934482564866)
XLA Ops:
  6.5 2.4 pad_maximum_fusion.2
  9.0 1.1 pad_maximum_fusion.3
  10.3 1.1 pad_maximum_fusion.4
  11.8 1.6 collective-permute-start
  13.3 1.3 dynamic_slice.20
  14.7 1.3 dynamic_slice.21
  16.0 0.6 multiply_exponential_fusion.2
  17.2 8.4 %collective-permute-done = bf16[1,128,2048]{2,1,0:T(8,128)(2,1)S(1)} collective-permute-done((bf16[1,128,2048]{2,1,0:T(8,128)(2,1)S(1)}, bf16[1,128,2048]{2,1,0:T(8,128)(2,1)S(1)}, u32[]{:S(2)}, u32[]{:S(2)}) %collective-permute-start) | collective-permute-done | bytes 524320 | tf_op jit(solution)/shard_map/ppermute | solution.py:33
  26.1 0.6 fusion.95
  26.7 1.2 fusion.99
  27.9 2.0 constant_dynamic-slice_fusion
  29.8 1.0 fusion.29
  30.8 1.2 fusion.28
  32.1 1.8 multiply_cosine_fusion
  34.2 98.8 %all-gather.4.cloned.1.call-done = bf16[2048,2048]{1,0:T(8,128)(2,1)} async-done(((bf16[256,2048]{1,0:T(8,128)(2,1)}), bf16[2048,2048]{1,0:T(8,128)(2,1)}) %all-gather.4.cloned.1.call-update) | async-done | bytes 8388624 | tf_op jit(solution)/shard_map/all_gather | solution.py:212
  133.0 8.1 %convolution_convert_fusion.1 = bf16[512,2048]{1,0:T(8,128)(2,1)S(1)} fusion(bf16[512,2048]{1,0:T(8,128)(2,1)S(1)} %bitcast.90, bf16[2048,2048]{1,0:T(8,128)(2,1)} %all-gather.4.cloned.1.call-done), kind=kOutput, calls=%fused_computation.33 | convolution fusion | flops 4296015872 | bytes 12582912 | tf_op jit(solution)/shard_map/dot_general | solution.py:223
  141.1 1.1 slice.296
  142.4 0.7 reshape.274
  143.1 0.7 reshape.276
  143.8 0.7 fusion.97
  145.1 1.3 copy-done.7
  146.4 1.5 convolution_convert_fusion.2
  147.9 2.5 collective-permute-start.2
  150.3 118.6 %all-gather.6.cloned.1.call-done = bf16[2048,2048]{1,0:T(8,128)(2,1)} async-done(((bf16[256,2048]{1,0:T(8,128)(2,1)}), bf16[2048,2048]{1,0:T(8,128)(2,1)}) %all-gather.6.cloned.1.call-update) | async-done | bytes 8388624 | tf_op jit(solution)/shard_map/all_gather | solution.py:212
  269.0 8.1 %convolution_convert_fusion = bf16[512,2048]{1,0:T(8,128)(2,1)S(1)} fusion(bf16[512,2048]{1,0:T(8,128)(2,1)S(1)} %bitcast.92, bf16[2048,2048]{1,0:T(8,128)(2,1)} %all-gather.6.cloned.1.call-done), kind=kOutput, calls=%fused_computation.32 | convolution fusion | flops 4296015872 | bytes 12582912 | tf_op jit(solution)/shard_map/dot_general | solution.py:223
  277.1 1.4 copy-done.4
  278.8 2.6 collective-permute-start.6
  281.4 4.6 fusion.11
  286.0 1.9 collective-permute-start.3
  288.0 5.5 %fusion.96 = (f32[512]{0:T(512)S(1)}, f32[512,512]{1,0:T(8,128)S(1)}) fusion(f32[512]{0:T(512)S(1)} %bitcast.109, bf16[512,512]{1,0:T(8,128)(2,1)S(1)} %multiply_convert_fusion.1, f32[512]{0:T(512)S(1)} %bitcast.111, bf16[30,512]{1,0:T(8,128)(2,1)S(1)} %collective-permute-done.6, f32[512]{0:T(512)S(1)} %bitcast.112, f32[512]{0:T(512)S(1)} %bitcast.113, ...), kind=kLoop, calls=%fused_computation.179 | loop fusion | flops 47971840 | bytes 1669120 | tf_op jit(solution)/shard_map/reduce_sum | solution.py:167
  293.4 32.7 %collective-permute-done.3 = bf16[2,256,512]{2,1,0:T(8,128)(2,1)S(1)} collective-permute-done((bf16[2,256,512]{2,1,0:T(8,128)(2,1)S(1)}, bf16[2,256,512]{2,1,0:T(8,128)(2,1)S(1)}, u32[]{:S(2)}, u32[]{:S(2)}) %collective-permute-start.3) | collective-permute-done | bytes 524320 | tf_op jit(solution)/shard_map/ppermute | solution.py:21
  326.2 0.9 fusion.34
  327.1 1.3 collective-permute-start.4
  328.7 29.1 %collective-permute-done.4 = bf16[2,256,512]{2,1,0:T(8,128)(2,1)S(1)} collective-permute-done((bf16[2,256,512]{2,1,0:T(8,128)(2,1)S(1)}, bf16[2,256,512]{2,1,0:T(8,128)(2,1)S(1)}, u32[]{:S(2)}, u32[]{:S(2)}) %collective-permute-start.4) | collective-permute-done | bytes 524320 | tf_op jit(solution)/shard_map/ppermute | solution.py:21
  357.8 1.2 fusion.43
  359.0 1.4 collective-permute-start.5
  360.4 71.5 %all-gather.8.cloned.1.call-done = bf16[2048,2048]{1,0:T(8,128)(2,1)} async-done(((bf16[256,2048]{1,0:T(8,128)(2,1)}), bf16[2048,2048]{1,0:T(8,128)(2,1)}) %all-gather.8.cloned.1.call-update) | async-done | bytes 8388624 | tf_op jit(solution)/shard_map/all_gather | solution.py:212
  431.9 4.8 fusion.30
  436.7 2.0 fusion.100
  439.2 1.9 copy.34
  441.1 2.6 fusion.10
  443.8 5.6 %fusion.2 = bf16[2,128,2048]{2,1,0:T(8,128)(2,1)} fusion(bf16[2048,2048]{1,0:T(8,128)(2,1)} %all-gather.8.cloned.1.call-done, bf16[2,2,128,1536]{3,2,1,0:T(8,128)(2,1)S(1)} %bitcast.93, s32[]{:T(128)S(6)} %select_n.70), kind=kOutput, calls=%fused_computation.36 | convolution fusion | flops 1611137024 | bytes 8126468 | tf_op jit(solution)/shard_map/dot_general | solution.py:175
  449.5 2.9 collective-permute-done.7
  452.3 4.6 convert_add_fusion
  456.9 1.3 copy-done.5
  458.4 1.5 collective-permute-start.8
  459.9 12.5 %collective-permute-done.8 = bf16[1,128,2048]{2,1,0:T(8,128)(2,1)S(1)} collective-permute-done((bf16[1,128,2048]{2,1,0:T(8,128)(2,1)S(1)}, bf16[1,128,2048]{2,1,0:T(8,128)(2,1)S(1)}, u32[]{:S(2)}, u32[]{:S(2)}) %collective-permute-start.8) | collective-permute-done | bytes 524320 | tf_op jit(solution)/shard_map/ppermute | solution.py:61
  472.4 2.1 fusion.44
  (85 shorter events, 4.3 us)
Async XLA Ops:
  6.5 2.4 copy-start.8
  6.5 2.5 copy-start.15
  6.5 2.5 copy-start.14
  6.5 126.5 %all-gather.4.cloned.1.call-start = ((), (), s32[]{:S(2)}) async-start(), calls=%async_computation | async-start | bytes 9437184 | tf_op jit(solution)/shard_map/all_gather | solution.py:212
  8.9 1.3 copy-start.9
  8.9 1.3 copy-start.16
  8.9 1.4 copy-start.17
  8.9 260.1 %all-gather.6.cloned.1.call-start = ((), (), s32[]{:S(2)}) async-start(), calls=%async_computation.1 | async-start | bytes 9437184 | tf_op jit(solution)/shard_map/all_gather | solution.py:212
  10.1 1.2 copy-start
  10.2 1.4 copy-start.18
  10.2 421.7 %all-gather.8.cloned.1.call-start = ((), (), s32[]{:S(2)}) async-start(), calls=%async_computation.2 | async-start | bytes 9437184 | tf_op jit(solution)/shard_map/all_gather | solution.py:212
  11.8 13.7 %collective-permute-start = (bf16[1,128,2048]{2,1,0:T(8,128)(2,1)S(1)}, bf16[1,128,2048]{2,1,0:T(8,128)(2,1)S(1)}, u32[]{:S(2)}, u32[]{:S(2)}) collective-permute-start(bf16[1,128,2048]{2,1,0:T(8,128)(2,1)S(1)} %fusion.45), channel_id=1, source_target_pairs={{0,2},{1,3},{2,0},{3,1},{4,6},{5,7},{6,4},{7,5},{8,10},{9,11},{10,... | collective-permute-start | bytes 1572872 | tf_op jit(solution)/shard_map/ppermute | solution.py:33
  16.0 16.0 %copy-start.24 = (f32[2]{0:T(128)}, f32[2]{0:T(128)S(1)}, u32[]{:S(2)}) copy-start(f32[2]{0:T(128)S(1)} %broadcast_multiply_fusion.2) | copy-start | bytes 28
  26.0 7.9 %collective-permute-start.1 = (bf16[2,128,2048]{2,1,0:T(8,128)(2,1)S(1)}, bf16[2,128,2048]{2,1,0:T(8,128)(2,1)S(1)}, u32[]{:S(2)}, u32[]{:S(2)}) collective-permute-start(bf16[2,128,2048]{2,1,0:T(8,128)(2,1)S(1)} %maximum_bitcast_fusion), channel_id=1, source_target_pairs={{0,1},{1,0},{2,3},{3,2},{4,5},{5,4},{6,7},{7,6},{8,9},{9,8},{10,11... | collective-permute-start | bytes 3145736 | tf_op jit(solution)/shard_map/ppermute | solution.py:33
  34.2 106.9 %copy-start.2 = (bf16[2,2,128,2048]{3,2,1,0:T(8,128)(2,1)}, bf16[2,2,128,2048]{3,2,1,0:T(8,128)(2,1)S(1)}, u32[]{:S(2)}) copy-start(bf16[2,2,128,2048]{3,2,1,0:T(8,128)(2,1)S(1)} %pad_maximum_fusion) | copy-start | bytes 6291460
  143.8 1.0 copy-start.6
  144.8 1.6 copy-start.7
  145.1 2.8 copy-start.11
  145.1 2.8 copy-start.12
  145.1 123.9 %copy-start.3 = (bf16[2,2,128,2048]{3,2,1,0:T(8,128)(2,1)S(1)}, bf16[2,2,128,2048]{3,2,1,0:T(8,128)(2,1)}, u32[]{:S(2)}) copy-start(bf16[2,2,128,2048]{3,2,1,0:T(8,128)(2,1)} %copy-done.2) | copy-start | bytes 6291460
  147.9 133.6 %copy-start.13 = (pred[512,512]{1,0:T(8,128)(4,1)S(1)}, pred[512,512]{1,0:T(8,128)(4,1)}, u32[]{:S(2)}) copy-start(pred[512,512]{1,0:T(8,128)(4,1)} %fusion.29) | copy-start | bytes 786436
  147.9 138.1 %collective-permute-start.2 = (bf16[2,256,512]{2,1,0:T(8,128)(2,1)}, bf16[2,256,512]{2,1,0:T(8,128)(2,1)S(1)}, u32[]{:S(2)}, u32[]{:S(2)}) collective-permute-start(bf16[2,256,512]{2,1,0:T(8,128)(2,1)} %convolution_convert_fusion.2), channel_id=1, source_target_pairs={{0,4},{4,8},{8,12},{12,16},{16,20},{20,24},{24,28},{1,5},{5,9},{9,... | collective-permute-start | bytes 1572872 | tf_op jit(solution)/shard_map/ppermute | solution.py:21
  277.1 1.4 copy-start.4
  278.8 9.2 %collective-permute-start.6 = (bf16[30,512]{1,0:T(8,128)(2,1)S(1)}, bf16[30,512]{1,0:T(8,128)(2,1)S(1)}, u32[]{:S(2)}, u32[]{:S(2)}) collective-permute-start(bf16[30,512]{1,0:T(8,128)(2,1)S(1)} %slice.306), channel_id=1, source_target_pairs={{0,4},{4,8},{8,12},{12,16},{16,20},{20,24},{24,28},{1,5},{5,9},{9,... | collective-permute-start | bytes 92168 | tf_op jit(solution)/shard_map/ppermute | solution.py:21
  286.0 40.2 %collective-permute-start.3 = (bf16[2,256,512]{2,1,0:T(8,128)(2,1)S(1)}, bf16[2,256,512]{2,1,0:T(8,128)(2,1)S(1)}, u32[]{:S(2)}, u32[]{:S(2)}) collective-permute-start(bf16[2,256,512]{2,1,0:T(8,128)(2,1)S(1)} %collective-permute-done.2), channel_id=1, source_target_pairs={{0,4},{4,8},{8,12},{12,16},{16,20},{20,24},{24,28},{1,5},{5,9},{9,... | collective-permute-start | bytes 1572872 | tf_op jit(solution)/shard_map/ppermute | solution.py:21
  287.9 69.9 %copy-start.19 = (f32[2]{0:T(128)S(1)}, f32[2]{0:T(128)}, u32[]{:S(2)}) copy-start(f32[2]{0:T(128)} %multiply_exponential_fusion.2) | copy-start | bytes 28
  287.9 69.9 %copy-start.22 = (f32[2]{0:T(128)S(1)}, f32[2]{0:T(128)}, u32[]{:S(2)}) copy-start(f32[2]{0:T(128)} %fusion.94) | copy-start | bytes 28
  293.4 138.5 %copy-start.20 = (f32[512]{0:T(512)S(1)}, f32[512]{0:T(512)}, u32[]{:S(2)}) copy-start(f32[512]{0:T(512)} %dynamic_slice.20) | copy-start | bytes 6148
  293.4 138.5 %copy-start.21 = (f32[512]{0:T(512)S(1)}, f32[512]{0:T(512)}, u32[]{:S(2)}) copy-start(f32[512]{0:T(512)} %dynamic_slice.21) | copy-start | bytes 6148
  327.1 30.7 %collective-permute-start.4 = (bf16[2,256,512]{2,1,0:T(8,128)(2,1)S(1)}, bf16[2,256,512]{2,1,0:T(8,128)(2,1)S(1)}, u32[]{:S(2)}, u32[]{:S(2)}) collective-permute-start(bf16[2,256,512]{2,1,0:T(8,128)(2,1)S(1)} %fusion.34), channel_id=1, source_target_pairs={{0,8},{4,12},{8,16},{12,20},{16,24},{20,28},{1,9},{5,13},{9,17},{1... | collective-permute-start | bytes 1572872 | tf_op jit(solution)/shard_map/ppermute | solution.py:21
  359.0 77.7 %copy-start.23 = (f32[2]{0:T(128)S(1)}, f32[2]{0:T(128)}, u32[]{:S(2)}) copy-start(f32[2]{0:T(128)} %fusion.95) | copy-start | bytes 28
  359.0 77.7 %collective-permute-start.5 = (bf16[2,256,512]{2,1,0:T(8,128)(2,1)}, bf16[2,256,512]{2,1,0:T(8,128)(2,1)}, u32[]{:S(2)}, u32[]{:S(2)}) collective-permute-start(bf16[2,256,512]{2,1,0:T(8,128)(2,1)} %fusion.43), channel_id=1, source_target_pairs={{0,16},{4,20},{8,24},{12,28},{1,17},{5,21},{9,25},{13,29},{2,18},{... | collective-permute-start | bytes 1572872 | tf_op jit(solution)/shard_map/ppermute | solution.py:21
  431.9 4.8 copy-start.1
  441.1 2.6 copy-start.10
  449.5 2.9 collective-permute-start.7
  456.9 1.4 copy-start.5
  458.4 14.0 %collective-permute-start.8 = (bf16[1,128,2048]{2,1,0:T(8,128)(2,1)S(1)}, bf16[1,128,2048]{2,1,0:T(8,128)(2,1)S(1)}, u32[]{:S(2)}, u32[]{:S(2)}) collective-permute-start(bf16[1,128,2048]{2,1,0:T(8,128)(2,1)S(1)} %dynamic-slice_convert_fusion), channel_id=1, source_target_pairs={{0,2},{1,3},{2,0},{3,1},{4,6},{5,7},{6,4},{7,5},{8,10},{9,11},{10,... | collective-permute-start | bytes 1572872 | tf_op jit(solution)/shard_map/ppermute | solution.py:61
Sparse Core Ops, SparseCore 0:
  9.5 123.5 all-gather.3
  135.1 133.8 all-gather.5
  271.1 160.7 all-gather.7

commit v3 on v2

--- a/solution.py
+++ b/solution.py
@@ -39,9 +39,10 @@
     return blocks.reshape((-1,) + x.shape[1:])
 
 
-def scatter_sums(make, hidden, axis):
-    size = lax.axis_size(axis)
+def scatter_sums(make, hidden, axis, pair_axis):
+    ranks = lax.axis_size(axis)
     rank = lax.axis_index(axis)
+    size = 2 * ranks
     rows = hidden.shape[0] // size
     parity = rank & 1
     paired = hidden.reshape(size // 2, 2, rows, hidden.shape[1])
@@ -55,22 +56,25 @@
     total = half(parity) + arrived.astype(jnp.float32)
     bit = 2
     while bit < size:
-        mine = (rank // bit) & 1
+        if bit < ranks:
+            mine, name, hop = (rank // bit) & 1, axis, bit
+        else:
+            mine, name, hop = lax.axis_index(pair_axis) & 1, pair_axis, 1
         split = total.reshape(-1, 2, rows, total.shape[-1])
         away = lax.dynamic_index_in_dim(split, 1 - mine, 1, False).astype(jnp.bfloat16)
-        arrived = lax.ppermute(away, axis, partners(axis, bit))
+        arrived = lax.ppermute(away, name, partners(name, hop))
         total = lax.dynamic_index_in_dim(split, mine, 1, False) + arrived.astype(jnp.float32)
         bit *= 2
     return total.reshape(rows, -1).astype(jnp.bfloat16)
 
 
 def state_before(contribution, totals, axis):
-    size = lax.axis_size(axis)
-    carried = from_behind(contribution.astype(jnp.bfloat16), axis, 1).astype(jnp.float32)
+    size = lax.axis_size(axis) // 2
+    carried = from_behind(contribution.astype(jnp.bfloat16), axis, 2).astype(jnp.float32)
     decay = totals
     reach = 1
     while reach < size - 1:
-        earlier = from_behind(carried.astype(jnp.bfloat16), axis, reach).astype(jnp.float32)
+        earlier = from_behind(carried.astype(jnp.bfloat16), axis, 2 * reach).astype(jnp.float32)
         carried = carried + decay[:, None, None] * earlier
         decay = decay * decay
         reach *= 2
@@ -163,10 +167,14 @@
             summed
             + padded[tap_index : tap_index + row_count].astype(jnp.float32) * tap_slice[tap_index]
         )
-    grouped = summed.reshape(row_count, -1, GROUP)
-    average = jnp.mean(grouped, axis=-1, keepdims=True)
-    spread = jnp.mean(jnp.square(grouped - average), axis=-1, keepdims=True)
-    normalized = ((grouped - average) * lax.rsqrt(spread + layer_eps)).reshape(row_count, -1)
+    def group_mean(x):
+        own = jnp.sum(x, axis=-1)
+        other = lax.ppermute(own, "sp", partners("sp", 1))
+        return ((own + other) / (2 * x.shape[1]))[:, None]
+
+    average = group_mean(summed)
+    spread = group_mean(jnp.square(summed - average))
+    normalized = (summed - average) * lax.rsqrt(spread + layer_eps)
     normalized = normalized * gain_slice + shift_slice
     return (jax.nn.silu(normalized) * jax.nn.silu(switch.astype(jnp.float32))).astype(jnp.bfloat16)
 
@@ -198,25 +206,38 @@
     head_rank = lax.axis_index("tp")
     chain_rank = lax.axis_index("sp")
     normed = rms_normalize(tokens, norm_gain)
-    in_weights = (
-        query_weight,
-        key_weight,
-        value_weight,
-        retain_gate,
-        unit_value,
-        unit_gate,
-        convolve_gate,
-    )
+    side = chain_rank & 1
+    pairs_total = chain_length // 2
+    lines = [[i for i in range(chain_length) if i % 2 == j] for j in range(2)]
+
+    def of_pair(own):
+        other = lax.ppermute(own, "sp", partners("sp", 1))
+        low = side == 0
+        return jnp.concatenate([jnp.where(low, own, other), jnp.where(low, other, own)], axis=0)
+
     def whole(*parts):
-        packed = jnp.concatenate(parts, axis=1)
-        return lax.all_gather(packed, "sp", axis=0, tiled=True)
-
-    first = whole(*in_weights[:3])
-    second = whole(*in_weights[3:6])
-    third = whole(in_weights[6], retain_output, convolve_output)
-    width = convolve_gate.shape[1]
-    out_full = third[:, width:]
-    rows = gather_rows(normed, "tp")
+        def packed(which):
+            return jnp.concatenate(
+                [
+                    lax.dynamic_slice_in_dim(m, which * (m.shape[1] // 2), m.shape[1] // 2, 1)
+                    for m in parts
+                ],
+                axis=1,
+            )
+
+        kept = packed(side)
+        arrived = lax.ppermute(packed(1 - side), "sp", partners("sp", 1))
+        low = side == 0
+        both = jnp.concatenate(
+            [jnp.where(low, kept, arrived), jnp.where(low, arrived, kept)], axis=0
+        )
+        return lax.all_gather(both, "sp", axis=0, tiled=True, axis_index_groups=lines)
+
+    first = whole(query_weight, key_weight, value_weight, unit_value, unit_gate)
+    second = whole(retain_gate, convolve_gate, retain_output, convolve_output)
+    rows = gather_rows(of_pair(normed), "tp")
+    rows = rows.reshape(head_groups, 2, -1, rows.shape[1]).swapaxes(0, 1)
+    rows = rows.reshape(-1, rows.shape[-1])
     row_count = rows.shape[0]
 
     def project(matrix, widths):
@@ -224,18 +245,25 @@
         bounds = [sum(widths[:i]) for i in range(len(widths) + 1)]
         return [made[:, bounds[i] : bounds[i + 1]] for i in range(len(widths))]
 
-    widths = [matrix.shape[1] for matrix in in_weights]
-    pieces = (
-        project(first, widths[:3])
-        + project(second, widths[3:6])
-        + project(third[:, :width], widths[6:])
-    )
-    queries, key_rows, values, retain_switch, glu_value, glu_switch, convolve_switch = pieces
+    early = (query_weight, key_weight, value_weight, unit_value, unit_gate)
+    late = (retain_gate, convolve_gate)
+    late_width = sum(m.shape[1] // 2 for m in late)
+    queries, key_rows, values, glu_value, glu_switch = project(
+        first, [m.shape[1] // 2 for m in early]
+    )
+    retain_switch, convolve_switch = project(
+        second[:, :late_width], [m.shape[1] // 2 for m in late]
+    )
+    out_full = second[:, late_width:]
     local_heads = queries.shape[1] // KEY
-    positions = chain_rank * row_count + jnp.arange(row_count, dtype=jnp.int32)
+    positions = (chain_rank // 2) * row_count + jnp.arange(row_count, dtype=jnp.int32)
     rotated_query, rotated_keys, value_heads = prepare(queries, key_rows, values, positions)
+    place = head_rank * 2 + side
     log_decay = decay_logs(
-        head_rank * local_heads, local_heads, local_heads * head_groups, row_count * chain_length
+        place * local_heads,
+        local_heads,
+        local_heads * head_groups * 2,
+        row_count * pairs_total,
     )
     within, contribution = local_parts(rotated_query, rotated_keys, value_heads, log_decay)
     totals = jnp.exp(log_decay * row_count)
@@ -243,18 +271,18 @@
         glu_value.astype(jnp.float32) * jax.nn.sigmoid(glu_switch.astype(jnp.float32))
     ).astype(jnp.bfloat16)
     channels = gated_input.shape[1]
-    before = from_behind(gated_input[row_count - (KW - 1) :], "sp", 1)
+    before = from_behind(gated_input[row_count - (KW - 1) :], "sp", 2)
     incoming = state_before(contribution, totals, "sp")
     raw = within + cross_part(rotated_query, incoming, log_decay)
     retain_hidden = retain_finish(raw, retain_switch)
-    tap_slice = lax.dynamic_slice_in_dim(filter_taps, head_rank * channels, channels, 1)
-    gain_slice = lax.dynamic_slice_in_dim(layer_gain, head_rank * channels, channels, 0)
-    shift_slice = lax.dynamic_slice_in_dim(layer_shift, head_rank * channels, channels, 0)
+    tap_slice = lax.dynamic_slice_in_dim(filter_taps, place * channels, channels, 1)
+    gain_slice = lax.dynamic_slice_in_dim(layer_gain, place * channels, channels, 0)
+    shift_slice = lax.dynamic_slice_in_dim(layer_shift, place * channels, channels, 0)
     convolve_hidden = convolve_branch(
         gated_input, before, tap_slice, gain_slice, shift_slice, convolve_switch
     )
     hidden = jnp.concatenate((retain_hidden, convolve_hidden), axis=1)
-    return scatter_sums(lambda rows: contract(rows, out_full), hidden, "tp")
+    return scatter_sums(lambda rows: contract(rows, out_full), hidden, "tp", "sp")
 
 
 def solution(mesh):

time: 482 us -> 368 us (0.76)
  waiting for transfers between devices: 375 us -> 266 us
  matrix products: 39.1 us -> 31.6 us
    all_gather x3 -> x2, waiting for transfers between devices: 289 us -> 143 us  [whole(): lax.all_gather(both, 'sp', axis=0, tiled=True, axis_index_groups=lines)]
    ppermute x1 -> x7, waiting for transfers between devices: 12.5 us -> 79.8 us  [the longest x2 36.5 us: scatter_sums(): arrived = lax.ppermute(away, name, partners(name, hop))]
    ppermute x5 -> x4, waiting for transfers between devices: 61.9 us -> 16 us  [from_behind(): return lax.ppermute(x, axis, pairs)]
    ppermute x2, waiting for transfers between devices: 8.36 us -> 22.5 us  [gather_rows(): other = lax.ppermute(blocks, axis, partners(axis, bit))]
    ppermute x1 -> x7, starting transfers between devices: 1.51 us -> 9.17 us  [the longest x2 3.49 us: group_mean(): other = lax.ppermute(own, 'sp', partners('sp', 1))]
    ppermute x5 -> x4, starting transfers between devices: 9.72 us -> 5.56 us  [from_behind(): return lax.ppermute(x, axis, pairs)]
    dot_general x3 -> x2, matrix products: 20.9 us -> 17.7 us  [project(): jnp.dot(rows, matrix, preferred_element_type=jnp.float32)]
  transfers between devices with their start and end apart: 12 -> 16, of which waited for: 8 -> 12; matrix products, arithmetic and copies ran while one was open for 11% -> 13% of each run, Pallas kernels for 0% -> 0%
where the time goes in v3:
time: 368 us; the launch traced here: 367 us
  waiting for transfers between devices  266 us (72%)
  matrix products  31.6 us (9%)
  other arithmetic  25.4 us (7%)
  starting transfers between devices  16.3 us (4%)
  between operations  13.9 us (4%)
  local copies, waits for them, and re-layouts  13.5 us (4%)
    all_gather x2, waiting for transfers between devices, whole(): lax.all_gather(both, 'sp', axis=0, tiled=True, axis_index_groups=lines)  143 us
    ppermute x2, waiting for transfers between devices, scatter_sums(): arrived = lax.ppermute(away, name, partners(name, hop))  36.5 us
    ppermute x2, waiting for transfers between devices, whole(): arrived = lax.ppermute(packed(1 - side), 'sp', partners('sp', 1))  35.7 us
    ppermute x2, waiting for transfers between devices, gather_rows(): other = lax.ppermute(blocks, axis, partners(axis, bit))  22.5 us
    dot_general x2, matrix products, project(): jnp.dot(rows, matrix, preferred_element_type=jnp.float32)  17.7 us
    ppermute x4, waiting for transfers between devices, from_behind(): return lax.ppermute(x, axis, pairs)  16 us
    ppermute x1, waiting for transfers between devices, of_pair(): other = lax.ppermute(own, 'sp', partners('sp', 1))  7.66 us
    dot_general x2, matrix products, contract(): lax.dot_general(hidden, matrix, (((1,), (1,)), ((), ())), preferred_eleme...  7.57 us
  transfers between devices with their start and end apart: 16, of which 12 were waited for; matrix products, arithmetic and copies ran while one was open for 13% of the time, Pallas kernels for 0%

profile of v3, /device:TPU:24, one launch (start us, length us, event | category | flops | bytes accessed | tf_op | source)
XLA Modules:
  0.0 366.9 jit_solution(9915854195065062480)
XLA Ops:
  6.5 1.0 dynamic-slice_dynamic-update-slice_fusion.9
  7.6 1.0 dynamic-slice_dynamic-update-slice_fusion.8
  8.6 1.3 dynamic-slice_dynamic-update-slice_fusion.1
  9.9 1.6 collective-permute-start.3
  11.5 17.8 %collective-permute-done.3 = bf16[256,1536]{1,0:T(8,128)(2,1)S(1)} collective-permute-done((bf16[256,1536]{1,0:T(8,128)(2,1)S(1)}, bf16[256,1536]{1,0:T(8,128)(2,1)S(1)}, u32[]{:S(2)}, u32[]{:S(2)}) %collective-permute-start.3) | collective-permute-done | bytes 786464 | tf_op jit(solution)/shard_map/ppermute | solution.py:229
  29.4 1.3 pad_maximum_fusion.1
  30.8 0.8 copy-done.8
  31.8 1.6 collective-permute-start.7
  34.4 17.9 %collective-permute-done.7 = bf16[256,1536]{1,0:T(8,128)(2,1)S(1)} collective-permute-done((bf16[256,1536]{1,0:T(8,128)(2,1)S(1)}, bf16[256,1536]{1,0:T(8,128)(2,1)S(1)}, u32[]{:S(2)}, u32[]{:S(2)}) %collective-permute-start.7) | collective-permute-done | bytes 786464 | tf_op jit(solution)/shard_map/ppermute | solution.py:229
  52.6 1.3 pad_maximum_fusion.2
  53.9 7.7 %collective-permute-done = bf16[128,2048]{1,0:T(8,128)(2,1)S(1)} collective-permute-done((bf16[128,2048]{1,0:T(8,128)(2,1)S(1)}, bf16[128,2048]{1,0:T(8,128)(2,1)S(1)}, u32[]{:S(2)}, u32[]{:S(2)}) %collective-permute-start) | collective-permute-done | bytes 524320 | tf_op jit(solution)/shard_map/ppermute | solution.py:214
  62.0 1.6 collective-permute-start.1
  63.6 21.9 %collective-permute-done.1 = bf16[1,256,2048]{2,1,0:T(8,128)(2,1)} collective-permute-done((bf16[1,256,2048]{2,1,0:T(8,128)(2,1)S(1)}, bf16[1,256,2048]{2,1,0:T(8,128)(2,1)}, u32[]{:S(2)}, u32[]{:S(2)}) %collective-permute-start.1) | collective-permute-done | bytes 1048608 | tf_op jit(solution)/shard_map/ppermute | solution.py:33
  85.5 1.8 select_bitcast_fusion.3
  87.2 1.5 maximum_bitcast_fusion
  90.4 1.1 fusion.106
  91.5 1.2 constant_dynamic-slice_fusion
  93.2 1.9 select_bitcast_fusion.1
  95.5 2.2 copy.20
  97.8 46.4 %all-gather.3.cloned.1.call-done = bf16[2048,1536]{1,0:T(8,128)(2,1)} async-done(((bf16[512,1536]{1,0:T(8,128)(2,1)}), bf16[2048,1536]{1,0:T(8,128)(2,1)}) %all-gather.3.cloned.1.call-update) | async-done | bytes 6291472 | tf_op jit(solution)/shard_map/all_gather | solution.py:234
  144.1 10.0 %convolution_convert_fusion = bf16[1024,1536]{1,0:T(8,128)(2,1)S(1)} fusion(bf16[1024,2048]{1,0:T(8,128)(2,1)} %bitcast.122, bf16[2048,1536]{1,0:T(8,128)(2,1)} %all-gather.3.cloned.1.call-done), kind=kOutput, calls=%fused_computation.37 | convolution fusion | flops 6444023808 | bytes 13631488 | tf_op jit(solution)/shard_map/dot_general | solution.py:244
  154.5 1.3 collective-permute-start.8
  155.9 3.1 fusion.47
  159.0 0.8 fusion.17
  159.8 1.5 collective-permute-start.4
  161.3 5.1 %fusion.105 = (f32[1024]{0:T(1024)S(1)}, f32[1024,256]{1,0:T(8,128)S(1)}) fusion(f32[256]{0:T(256)S(1)} %bitcast.140, bf16[1024,256]{1,0:T(8,128)(2,1)S(1)} %multiply_convert_fusion, f32[256]{0:T(256)S(1)} %bitcast.142, bf16[30,256]{1,0:T(8,128)(2,1)S(1)} %collective-permute-done.8, f32[256]{0:T(256)S(1)} %bitcast.143, f32[256]{0:T(256)S(1)} %bitcast.144, ...), kind=kLoop, calls=%fused_computation.207 | loop fusion | flops 47971328 | bytes 1624064 | tf_op jit(solution)/shard_map/reduce_sum | solution.py:171
  166.4 1.7 collective-permute-start.9
  168.2 96.9 %all-gather.5.cloned.1.call-done = bf16[2048,1536]{1,0:T(8,128)(2,1)} async-done(((bf16[512,1536]{1,0:T(8,128)(2,1)}), bf16[2048,1536]{1,0:T(8,128)(2,1)}) %all-gather.5.cloned.1.call-update) | async-done | bytes 6291472 | tf_op jit(solution)/shard_map/all_gather | solution.py:234
  265.1 7.7 %fusion.13 = bf16[1024,768]{1,0:T(8,128)(2,1)} fusion(bf16[1024,2048]{1,0:T(8,128)(2,1)} %bitcast.123, bf16[2048,1536]{1,0:T(8,128)(2,1)} %all-gather.5.cloned.1.call-done), kind=kOutput, calls=%fused_computation.58 | convolution fusion | flops 3222011904 | bytes 8912896 | tf_op jit(solution)/shard_map/dot_general | solution.py:244
  273.2 1.7 collective-permute-start.10
  274.9 1.3 collective-permute-start.5
  276.2 3.9 %fusion.16 = f32[512,1024]{0,1:T(8,128)S(1)} fusion(f32[]{:T(128)S(6)} %div.61, bf16[1024,1536]{1,0:T(8,128)(2,1)} %copy-done.3, bf16[1024,128]{1,0:T(8,128)(2,1)S(1)} %get-tuple-element.72, bf16[1024,128]{1,0:T(8,128)(2,1)} %get-tuple-element.73, f32[1024,128]{1,0:T(8,128)} %copy-done.6, f32[1024,128]{1,0:T(8,128)} %copy-done.5), kind=kOutput, calls=%fused_computation.62 | convolution fusion | flops 1619787776 | bytes 4718596 | tf_op jit(solution)/shard_map/hij,jhe->ihe/dot_general | solution.py:132
  280.1 4.9 %collective-permute-done.5 = bf16[1,256,512]{2,1,0:T(8,128)(2,1)} collective-permute-done((bf16[1,256,512]{2,1,0:T(8,128)(2,1)}, bf16[1,256,512]{2,1,0:T(8,128)(2,1)}, u32[]{:S(2)}, u32[]{:S(2)}) %collective-permute-start.5) | collective-permute-done | bytes 262176 | tf_op jit(solution)/shard_map/ppermute | solution.py:21
  285.0 1.1 fusion.83
  286.2 1.5 collective-permute-start.6
  287.7 1.8 fusion.27
  289.5 11.1 %collective-permute-done.6 = bf16[1,256,512]{2,1,0:T(8,128)(2,1)S(1)} collective-permute-done((bf16[1,256,512]{2,1,0:T(8,128)(2,1)S(1)}, bf16[1,256,512]{2,1,0:T(8,128)(2,1)S(1)}, u32[]{:S(2)}, u32[]{:S(2)}) %collective-permute-start.6) | collective-permute-done | bytes 262176 | tf_op jit(solution)/shard_map/ppermute | solution.py:21
  300.6 1.7 fusion.107
  302.8 0.9 copy-done.2
  304.6 3.2 convolution_convert_fusion.1
  307.8 4.5 %collective-permute-done.11 = bf16[4,128,2048]{2,1,0:T(8,128)(2,1)} collective-permute-done((bf16[4,128,2048]{2,1,0:T(8,128)(2,1)}, bf16[4,128,2048]{2,1,0:T(8,128)(2,1)}, u32[]{:S(2)}, u32[]{:S(2)}) %collective-permute-start.11) | collective-permute-done | bytes 2097184 | tf_op jit(solution)/shard_map/ppermute | solution.py:55
  312.3 4.4 %convert_add_fusion = f32[4,128,2048]{2,1,0:T(8,128)S(1)} fusion(bf16[4,128,2048]{2,1,0:T(8,128)(2,1)} %collective-permute-done.11, bf16[2048,1536]{1,0:T(8,128)(2,1)} %all-gather.5.cloned.1.call-done, bf16[4,2,128,768]{3,2,1,0:T(8,128)(2,1)S(1)} %bitcast.127, s32[]{:T(128)S(6)} %select_n.147), kind=kOutput, calls=%fused_computation.36 | convolution fusion | flops 1612709888 | bytes 10223620 | tf_op jit(solution)/shard_map/dot_general | solution.py:183
  316.7 2.0 copy-done.1
  318.8 1.5 collective-permute-start.12
  320.3 23.7 %collective-permute-done.12 = bf16[2,128,2048]{2,1,0:T(8,128)(2,1)S(1)} collective-permute-done((bf16[2,128,2048]{2,1,0:T(8,128)(2,1)S(1)}, bf16[2,128,2048]{2,1,0:T(8,128)(2,1)S(1)}, u32[]{:S(2)}, u32[]{:S(2)}) %collective-permute-start.12) | collective-permute-done | bytes 1048608 | tf_op jit(solution)/shard_map/ppermute | solution.py:65
  344.1 1.8 bitcast_add_fusion
  346.4 12.8 %collective-permute-done.13 = bf16[1,128,2048]{2,1,0:T(8,128)(2,1)S(1)} collective-permute-done((bf16[1,128,2048]{2,1,0:T(8,128)(2,1)S(1)}, bf16[1,128,2048]{2,1,0:T(8,128)(2,1)S(1)}, u32[]{:S(2)}, u32[]{:S(2)}) %collective-permute-start.13) | collective-permute-done | bytes 524320 | tf_op jit(solution)/shard_map/ppermute | solution.py:65
  359.2 0.9 fusion.50
  (73 shorter events, 7.5 us)
Async XLA Ops:
  6.5 3.3 copy-start.10
  6.5 3.4 copy-start.11
  6.5 137.6 %all-gather.3.cloned.1.call-start = ((), (), s32[]{:S(2)}) async-start(), calls=%async_computation | async-start | bytes 7864320 | tf_op jit(solution)/shard_map/all_gather | solution.py:234
  9.9 19.3 %collective-permute-start.3 = (bf16[256,1536]{1,0:T(8,128)(2,1)S(1)}, bf16[256,1536]{1,0:T(8,128)(2,1)S(1)}, u32[]{:S(2)}, u32[]{:S(2)}) collective-permute-start(bf16[256,1536]{1,0:T(8,128)(2,1)S(1)} %get-tuple-element.61), channel_id=1, source_target_pairs={{0,4},{4,0},{8,12},{12,8},{16,20},{20,16},{24,28},{28,24},{1,5},{5... | collective-permute-start | bytes 2359304 | tf_op jit(solution)/shard_map/ppermute | solution.py:229
  29.4 1.4 copy-start.7
  30.7 0.9 copy-start.8
  30.7 1.0 copy-start.9
  30.7 2.7 copy-start
  30.7 2.9 copy-start.12
  30.7 234.3 %all-gather.5.cloned.1.call-start = ((), (), s32[]{:S(2)}) async-start(), calls=%async_computation.1 | async-start | bytes 7864320 | tf_op jit(solution)/shard_map/all_gather | solution.py:234
  31.8 20.5 %collective-permute-start.7 = (bf16[256,1536]{1,0:T(8,128)(2,1)S(1)}, bf16[256,1536]{1,0:T(8,128)(2,1)S(1)}, u32[]{:S(2)}, u32[]{:S(2)}) collective-permute-start(bf16[256,1536]{1,0:T(8,128)(2,1)S(1)} %pad_maximum_fusion.5), channel_id=1, source_target_pairs={{0,4},{4,0},{8,12},{12,8},{16,20},{20,16},{24,28},{28,24},{1,5},{5... | collective-permute-start | bytes 2359304 | tf_op jit(solution)/shard_map/ppermute | solution.py:229
  33.8 27.7 %collective-permute-start = (bf16[128,2048]{1,0:T(8,128)(2,1)S(1)}, bf16[128,2048]{1,0:T(8,128)(2,1)S(1)}, u32[]{:S(2)}, u32[]{:S(2)}) collective-permute-start(bf16[128,2048]{1,0:T(8,128)(2,1)S(1)} %fusion.20), channel_id=1, source_target_pairs={{0,4},{4,0},{8,12},{12,8},{16,20},{20,16},{24,28},{28,24},{1,5},{5... | collective-permute-start | bytes 1572872 | tf_op jit(solution)/shard_map/ppermute | solution.py:214
  62.0 23.5 %collective-permute-start.1 = (bf16[1,256,2048]{2,1,0:T(8,128)(2,1)S(1)}, bf16[1,256,2048]{2,1,0:T(8,128)(2,1)}, u32[]{:S(2)}, u32[]{:S(2)}) collective-permute-start(bf16[1,256,2048]{2,1,0:T(8,128)(2,1)S(1)} %maximum_bitcast_fusion.1), channel_id=1, source_target_pairs={{0,2},{1,3},{2,0},{3,1},{4,6},{5,7},{6,4},{7,5},{8,10},{9,11},{10,... | collective-permute-start | bytes 3145736 | tf_op jit(solution)/shard_map/ppermute | solution.py:33
  88.7 4.5 %collective-permute-start.2 = (bf16[2,256,2048]{2,1,0:T(8,128)(2,1)}, bf16[2,256,2048]{2,1,0:T(8,128)(2,1)}, u32[]{:S(2)}, u32[]{:S(2)}) collective-permute-start(bf16[2,256,2048]{2,1,0:T(8,128)(2,1)} %maximum_bitcast_fusion), channel_id=1, source_target_pairs={{0,1},{1,0},{2,3},{3,2},{4,5},{5,4},{6,7},{7,6},{8,9},{9,8},{10,11... | collective-permute-start | bytes 6291464 | tf_op jit(solution)/shard_map/ppermute | solution.py:33
  154.1 4.9 %copy-start.3 = (bf16[1024,1536]{1,0:T(8,128)(2,1)}, bf16[1024,1536]{1,0:T(8,128)(2,1)S(1)}, u32[]{:S(2)}) copy-start(bf16[1024,1536]{1,0:T(8,128)(2,1)S(1)} %convolution_convert_fusion) | copy-start | bytes 9437188
  154.5 6.8 %collective-permute-start.8 = (bf16[30,256]{1,0:T(8,128)(2,1)S(1)}, bf16[30,256]{1,0:T(8,128)(2,1)S(1)}, u32[]{:S(2)}, u32[]{:S(2)}) collective-permute-start(bf16[30,256]{1,0:T(8,128)(2,1)S(1)} %slice.311), channel_id=1, source_target_pairs={{0,8},{4,12},{8,16},{12,20},{16,24},{20,28},{1,9},{5,13},{9,17},{1... | collective-permute-start | bytes 46088 | tf_op jit(solution)/shard_map/ppermute | solution.py:21
  159.0 2.3 copy-start.5
  159.0 2.3 copy-start.6
  159.8 115.1 %collective-permute-start.4 = (bf16[1,256,512]{2,1,0:T(8,128)(2,1)S(1)}, bf16[1,256,512]{2,1,0:T(8,128)(2,1)}, u32[]{:S(2)}, u32[]{:S(2)}) collective-permute-start(bf16[1,256,512]{2,1,0:T(8,128)(2,1)S(1)} %fusion.17), channel_id=1, source_target_pairs={{0,8},{4,12},{8,16},{12,20},{16,24},{20,28},{1,9},{5,13},{9,17},{1... | collective-permute-start | bytes 786440 | tf_op jit(solution)/shard_map/ppermute | solution.py:21
  166.4 106.4 %collective-permute-start.9 = (f32[1024]{0:T(1024)S(1)}, f32[1024]{0:T(1024)S(1)}, u32[]{:S(2)}, u32[]{:S(2)}) collective-permute-start(f32[1024]{0:T(1024)S(1)} %get-tuple-element.5), channel_id=1, source_target_pairs={{0,4},{4,0},{8,12},{12,8},{16,20},{20,16},{24,28},{28,24},{1,5},{5... | collective-permute-start | bytes 12296 | tf_op jit(solution)/shard_map/ppermute | solution.py:172
  273.2 6.9 %collective-permute-start.10 = (f32[1024]{0:T(1024)S(1)}, f32[1024]{0:T(1024)S(1)}, u32[]{:S(2)}, u32[]{:S(2)}) collective-permute-start(f32[1024]{0:T(1024)S(1)} %multiply_reduce_fusion.1), channel_id=1, source_target_pairs={{0,4},{4,0},{8,12},{12,8},{16,20},{20,16},{24,28},{28,24},{1,5},{5... | collective-permute-start | bytes 12296 | tf_op jit(solution)/shard_map/ppermute | solution.py:172
  274.9 10.1 %collective-permute-start.5 = (bf16[1,256,512]{2,1,0:T(8,128)(2,1)}, bf16[1,256,512]{2,1,0:T(8,128)(2,1)}, u32[]{:S(2)}, u32[]{:S(2)}) collective-permute-start(bf16[1,256,512]{2,1,0:T(8,128)(2,1)} %collective-permute-done.4), channel_id=1, source_target_pairs={{0,8},{4,12},{8,16},{12,20},{16,24},{20,28},{1,9},{5,13},{9,17},{1... | collective-permute-start | bytes 786440 | tf_op jit(solution)/shard_map/ppermute | solution.py:21
  280.1 20.5 %copy-start.4 = (bf16[1024,128]{1,0:T(8,128)(2,1)S(1)}, bf16[1024,128]{1,0:T(8,128)(2,1)}, u32[]{:S(2)}) copy-start(bf16[1024,128]{1,0:T(8,128)(2,1)} %get-tuple-element.73) | copy-start | bytes 786436
  286.2 14.5 %collective-permute-start.6 = (bf16[1,256,512]{2,1,0:T(8,128)(2,1)S(1)}, bf16[1,256,512]{2,1,0:T(8,128)(2,1)S(1)}, u32[]{:S(2)}, u32[]{:S(2)}) collective-permute-start(bf16[1,256,512]{2,1,0:T(8,128)(2,1)S(1)} %fusion.83), channel_id=1, source_target_pairs={{0,16},{4,20},{8,24},{12,28},{1,17},{5,21},{9,25},{13,29},{2,18},{... | collective-permute-start | bytes 786440 | tf_op jit(solution)/shard_map/ppermute | solution.py:21
  287.7 16.9 %slice-start = ((s8[6291456]{0:T(1024)(128)(4,1)}), s8[4194304]{0:T(1024)(128)(4,1)S(1)}, s32[]{:S(2)}) async-start(s8[6291456]{0:T(1024)(128)(4,1)} %bitcast.159), calls=%async_computation.2 | async-start | bytes 8388608
  302.3 1.4 copy-start.2
  302.3 2.2 slice-start.1
  307.8 4.5 %collective-permute-start.11 = (bf16[4,128,2048]{2,1,0:T(8,128)(2,1)}, bf16[4,128,2048]{2,1,0:T(8,128)(2,1)}, u32[]{:S(2)}, u32[]{:S(2)}) collective-permute-start(bf16[4,128,2048]{2,1,0:T(8,128)(2,1)} %convolution_convert_fusion.1), channel_id=1, source_target_pairs={{0,1},{1,0},{2,3},{3,2},{4,5},{5,4},{6,7},{7,6},{8,9},{9,8},{10,11... | collective-permute-start | bytes 6291464 | tf_op jit(solution)/shard_map/ppermute | solution.py:55
  316.7 2.0 copy-start.1
  318.8 25.3 %collective-permute-start.12 = (bf16[2,128,2048]{2,1,0:T(8,128)(2,1)S(1)}, bf16[2,128,2048]{2,1,0:T(8,128)(2,1)S(1)}, u32[]{:S(2)}, u32[]{:S(2)}) collective-permute-start(bf16[2,128,2048]{2,1,0:T(8,128)(2,1)S(1)} %fusion.25), channel_id=1, source_target_pairs={{0,2},{1,3},{2,0},{3,1},{4,6},{5,7},{6,4},{7,5},{8,10},{9,11},{10,... | collective-permute-start | bytes 3145736 | tf_op jit(solution)/shard_map/ppermute | solution.py:65
  346.0 13.2 %collective-permute-start.13 = (bf16[1,128,2048]{2,1,0:T(8,128)(2,1)S(1)}, bf16[1,128,2048]{2,1,0:T(8,128)(2,1)S(1)}, u32[]{:S(2)}, u32[]{:S(2)}) collective-permute-start(bf16[1,128,2048]{2,1,0:T(8,128)(2,1)S(1)} %dynamic-slice_convert_fusion), channel_id=1, source_target_pairs={{0,4},{4,0},{8,12},{12,8},{16,20},{20,16},{24,28},{28,24},{1,5},{5... | collective-permute-start | bytes 1572872 | tf_op jit(solution)/shard_map/ppermute | solution.py:65
Sparse Core Ops, SparseCore 0:
  30.8 113.2 all-gather.2
  145.7 119.3 all-gather.4
